TPU v7x, 256 devices: a 4x2x16 block of a 4x16x16 slice. The times are simulated.
256 devices in a mesh: grp: 2 (over y), sp: 32 (over z, core), tp: 4 (over x).
Axes of the slice: x: 4, y: 2, z: 16, core: 2. Of those that a mesh axis runs over, the one named last changes fastest.
The devices are a block of a 4x16x16 slice.
Arguments:
- query_rows: bfloat16 [8192, 1024], P(('grp', 'sp'), 'tp'), parts along dimension 0, may hold values from -6 to 6
- key_rows: bfloat16 [8192, 1024], P(('grp', 'sp'), 'tp'), parts along dimension 0, may hold values from -6 to 6
- value_rows: bfloat16 [8192, 1024], P(('grp', 'sp'), 'tp'), parts along dimension 0, may hold values from -6 to 6
- gate_rows: bfloat16 [8192, 1024], P(('grp', 'sp'), 'tp'), parts along dimension 0, may hold values from -6 to 6
- log_decay: float32 [2, 8, 8192], P(None, 'tp', ('grp', 'sp')), parts along dimension 2, may hold values from -2 to 0, as said below
- head_gain: float32 [2, 1024], P(None, 'tp'), may hold values from 0.1 to 1.9
- out_weight: bfloat16 [1024, 2048], P('tp'), may hold values from -0.1875 to 0.1875
- residual: bfloat16 [8192, 2048], P(('grp', 'sp')), parts along dimension 0, may hold values from -6 to 6
- norm_gain: bfloat16 [2048], replicated, may hold values from 0.099609375 to 1.8984375
- gate_weight: bfloat16 [2048, 5632], P('sp', 'tp'), may hold values from -0.125 to 0.125
- up_weight: bfloat16 [2048, 5632], P('sp', 'tp'), may hold values from -0.125 to 0.125
- down_weight: bfloat16 [2048, 5632], P('sp', 'tp'), may hold values from -0.078125 to 0.078125
- gate_taps: bfloat16 [3, 5632], P(None, 'tp'), may hold values from -3.5 to 3.5
- up_taps: bfloat16 [3, 5632], P(None, 'tp'), may hold values from -3.5 to 3.5
Outputs:
- block_out: bfloat16 [8192, 2048], P(('grp', 'sp', 'tp')), parts along dimension 0
There are 2 independent parts, one for each index of `grp`. A program takes and returns all parts, laid end to end along the dimension named above; an argument that names none is the same for every part. Nothing has to cross between parts.
Inputs may be any that keep to these rules, and one draw needn't show every extreme that they name: `log_decay`: every entry is negative.
All inputs are finite; a program needn't handle non-finite values.
Results may differ from a plain program's by a relative error of at most 0.017.
Values may be sent and summed in bfloat16 or wider, within the bound.
No kernel may reach another device: no remote copies, remote signals or barrier semaphores. Data moves between devices by JAX's collectives and lax.ppermute only.
A program may use at most 64 MiB of HBM per device.

v0:
```python
import math

import jax
import jax.numpy as jnp
from jax import lax
from jax.sharding import Mesh
from jax.sharding import PartitionSpec as P

HEAD = 128
SP = ("sp_0", "sp_1")
GRP_SP = ("grp", "sp_0", "sp_1")
GRP_SP_TP = ("grp", "sp_0", "sp_1", "tp")


GROUP_EPS = 1e-05
NORM_EPS = 1e-06


def nothing_yet(shard, identity):
    return jax.tree.map(
        lambda a, e: jnp.broadcast_to(jnp.asarray(e, a.dtype), a.shape), shard, identity
    )


def entering_2(shard, axes, combine, identity, reverse):
    before = start = nothing_yet(shard, identity)
    running = shard
    for axis in reversed(axes):
        length, index = (lax.axis_size(axis), lax.axis_index(axis))
        pieces = jax.tree.map(lambda part: lax.all_gather(part, axis), running)
        inside, running = (start, start)
        for k in reversed(range(length)) if reverse else range(length):
            passed = k > index if reverse else k < index
            running = combine(running, jax.tree.map(lambda part: part[k], pieces))
            inside = jax.tree.map(lambda new, old: jnp.where(passed, new, old), running, inside)
        before = combine(inside, before)
    return before


def sent_together(arrays, axis, dim, along):
    ends, at = ([], 0)
    for a in arrays[:-1]:
        at += a.shape[along]
        ends.append(at)
    both = jnp.concatenate(arrays, axis=along)
    return tuple(jnp.split(lax.all_gather(both, axis, axis=dim, tiled=True), ends, axis=along))


def cut_along(shard, dim, length):
    shape = shard.shape
    parts = shard.reshape(*shape[:dim], length, shape[dim] // length, *shape[dim + 1 :])
    return jnp.moveaxis(parts, dim, 0)


def summed_on_arrival(shard, axis, dim):
    parts = cut_along(shard, dim, lax.axis_size(axis))
    arrived = lax.all_to_all(parts, axis, split_axis=0, concat_axis=0, tiled=True)
    return arrived.astype(jnp.float32).sum(axis=0)


def sent_to_all(shard, axis):
    length = lax.axis_size(axis)
    return lax.all_to_all(
        jnp.broadcast_to(shard[None], (length, *shard.shape)), axis, 0, 0, tiled=True
    )


def laid_out(parts, dim):
    parts = jnp.moveaxis(parts, 0, dim)
    shape = parts.shape
    return parts.reshape(*shape[:dim], shape[dim] * shape[dim + 1], *shape[dim + 2 :])


def gathered_copies(shard, axis, dim):
    parts = sent_to_all(shard, axis)
    return laid_out(parts, dim)


def padded_2(shard, sides, width):
    for axis, dim in sides:
        size, length = (lax.axis_size(axis), shard.shape[dim])
        up = [(i, (i + 1) % size) for i in range(size - 1)]
        down = [(j, i) for i, j in up]
        last = lax.slice_in_dim(shard, length - width, length, axis=dim)
        initial = lax.slice_in_dim(shard, 0, width, axis=dim)
        before = lax.ppermute(last, axis, up)
        after = lax.ppermute(initial, axis, down)
        shard = jnp.concatenate([before, shard, after], axis=dim)
    return shard


def state_combine(earlier, later):
    return (earlier[0] * later[0], earlier[1] * later[0][:, None, None] + later[1])


def group_norm(values):
    length, head_count, head_width = values.shape
    centre = values - jnp.mean(values, axis=2, keepdims=True)
    spread = jnp.mean(centre * centre, axis=2, keepdims=True)
    return (centre * lax.rsqrt(spread + GROUP_EPS)).reshape(length, head_count * head_width)


def rms_scale(middle, gain):
    values = middle.astype(jnp.float32)
    multiplier = lax.rsqrt(jnp.mean(values * values, axis=1, keepdims=True) + NORM_EPS)
    return (values * multiplier * gain.astype(jnp.float32)).astype(jnp.bfloat16)


def local_retention(query_all, key_all, value_all, log_rates):
    length, head_count, head_width = query_all.shape
    block_len = math.gcd(length, 512)
    block_count = length // block_len
    cumul = jnp.cumsum(log_rates, axis=1).T
    query_block = query_all.reshape(block_count, block_len, head_count, head_width)
    key_block = key_all.reshape(block_count, block_len, head_count, head_width)
    value_block = value_all.reshape(block_count, block_len, head_count, head_width)
    cumul_block = cumul.reshape(block_count, block_len, head_count)
    before = jnp.concatenate(
        [jnp.zeros((1, head_count), jnp.float32), cumul_block[:-1, -1]], axis=0
    )
    local_cumul = cumul_block - before[:, None, :]
    gap_logs = local_cumul[:, :, None, :] - local_cumul[:, None, :, :]
    lower_mask = (jnp.arange(block_len)[:, None] >= jnp.arange(block_len)[None, :])[
        None, :, :, None
    ]
    decay_mask = jnp.where(lower_mask, jnp.exp(jnp.minimum(gap_logs, 0.0)), 0.0)
    scores = jnp.einsum("bthd,bshd->btsh", query_block, key_block) * decay_mask
    inner_part = jnp.einsum("btsh,bshe->bthe", scores, value_block)
    to_end = jnp.exp(local_cumul[:, -1:, :] - local_cumul)
    block_states = jnp.einsum("bshd,bshe->bhde", key_block * to_end[..., None], value_block)
    block_decay = jnp.exp(local_cumul[:, -1, :])

    def carry_step(carry_state, inputs):
        return (carry_state * inputs[0][:, None, None] + inputs[1], carry_state)

    zero_state = jnp.zeros((head_count, head_width, head_width), jnp.float32)
    end_state, entering = lax.scan(carry_step, zero_state, (block_decay, block_states))
    carried = jnp.einsum("bthd,bhde->bthe", query_block * jnp.exp(local_cumul)[..., None], entering)
    output = (inner_part + carried).reshape(length, head_count, head_width)
    return (output, end_state, cumul, jnp.exp(cumul[-1]))


def with_incoming(output, query_all, cumul, incoming):
    return output + jnp.einsum("thd,hde->the", query_all * jnp.exp(cumul)[:, :, None], incoming)


def shards(
    query_rows,
    key_rows,
    value_rows,
    gate_rows,
    log_decay,
    head_gain,
    out_weight,
    residual,
    norm_gain,
    gate_weight,
    up_weight,
    down_weight,
    gate_taps,
    up_taps,
):
    pair_local = jnp.concatenate([gate_weight, up_weight], axis=1)
    row_count = query_rows.shape[0]
    head_count = query_rows.shape[1] // HEAD
    key_scale = HEAD ** (-0.5)
    query_all = query_rows.astype(jnp.float32).reshape(row_count, head_count, HEAD)
    key_all = key_rows.astype(jnp.float32).reshape(row_count, head_count, HEAD) * key_scale
    value_all = value_rows.astype(jnp.float32).reshape(row_count, head_count, HEAD)
    identity = (
        jnp.ones((head_count,), jnp.float32),
        jnp.zeros((head_count, HEAD, HEAD), jnp.float32),
    )
    ahead_local, ahead_state, ahead_cumul, ahead_decay = local_retention(
        query_all, key_all, value_all, log_decay[0]
    )
    query_back = query_all[::-1]
    behind_local, behind_state, behind_cumul, behind_decay = local_retention(
        query_back, key_all[::-1], value_all[::-1], log_decay[1][:, ::-1]
    )
    ahead_in = entering_2((ahead_decay, ahead_state), SP, state_combine, identity, False)[1]
    behind_in = entering_2((behind_decay, behind_state), SP, state_combine, identity, True)[1]
    ahead_out = with_incoming(ahead_local, query_all, ahead_cumul, ahead_in)
    behind_out = with_incoming(behind_local, query_back, behind_cumul, behind_in)[::-1]
    combined = group_norm(ahead_out) * head_gain[0] + group_norm(behind_out) * head_gain[1]
    mixed_heads = (jax.nn.silu(gate_rows.astype(jnp.float32)) * combined).astype(jnp.bfloat16)
    gathered = sent_together((pair_local, down_weight), SP, 0, 1)
    pair_full, down_full = gathered
    share_rows = row_count // lax.axis_size("tp")
    own_start = lax.axis_index("tp") * share_rows
    picked = mixed_heads
    attended = summed_on_arrival(
        jnp.dot(picked, out_weight, preferred_element_type=jnp.float32).astype(jnp.bfloat16),
        "tp",
        0,
    )
    residual_own = lax.dynamic_slice_in_dim(residual, own_start, share_rows, 0)
    middle_own = lax.optimization_barrier(
        (residual_own.astype(jnp.float32) + attended).astype(jnp.bfloat16)
    )
    normed = rms_scale(middle_own, norm_gain)
    pre_both = jnp.dot(
        gathered_copies(normed, "tp", 0), pair_full, preferred_element_type=jnp.float32
    ).astype(jnp.bfloat16)
    padded = padded_2(pre_both, ((SP, 0),), 1)
    half_width = gate_taps.shape[1]
    tap_table = jnp.concatenate([gate_taps, up_taps], axis=1).astype(jnp.float32)
    conv_out = (
        tap_table[0] * padded[:-2].astype(jnp.float32)
        + tap_table[1] * padded[1:-1].astype(jnp.float32)
        + tap_table[2] * padded[2:].astype(jnp.float32)
    )
    hidden = (jax.nn.silu(conv_out[:, :half_width]) * conv_out[:, half_width:]).astype(jnp.bfloat16)
    picked = hidden
    ff_out = summed_on_arrival(
        lax.dot_general(
            picked, down_full, (((1,), (1,)), ((), ())), preferred_element_type=jnp.float32
        ).astype(jnp.bfloat16),
        "tp",
        0,
    )
    return (middle_own.astype(jnp.float32) + ff_out).astype(jnp.bfloat16)


def solution(mesh):
    split = Mesh(
        mesh.devices.reshape(mesh.shape["grp"], 16, 2, mesh.shape["tp"]),
        ("grp", "sp_0", "sp_1", "tp"),
    )
    placed = (
        P(GRP_SP, "tp"),
        P(GRP_SP, "tp"),
        P(GRP_SP, "tp"),
        P(GRP_SP, "tp"),
        P(None, "tp", GRP_SP),
        P(None, "tp"),
        P("tp", None),
        P(GRP_SP, None),
        P(),
        P(SP, "tp"),
        P(SP, "tp"),
        P(SP, "tp"),
        P(None, "tp"),
        P(None, "tp"),
    )
    return jax.shard_map(
        shards, mesh=split, in_specs=placed, out_specs=P(GRP_SP_TP, None), check_vma=False
    )
```

profile of v0, /device:TPU:33, one launch (start us, length us, event | category | flops | bytes accessed | tf_op | source)
XLA Modules:
  0.0 316.0 jit_solution(3661982202352808028)
XLA Ops:
  6.6 0.8 slice_bitcast_fusion.33
  7.3 0.1 rev.17
  7.4 0.3 reduce_window_sum.18
  7.8 0.2 slice_reduce_fusion
  7.9 0.1 bitcast_exponential_fusion
  8.0 0.2 exponential_reduce_fusion
  8.2 21.9 %all-gather.4 = f32[2,1,2]{2,1,0:T(1,128)S(1)} all-gather(f32[1,1,2]{2,1,0:T(1,128)S(1)} %bitcast.498), channel_id=1, replica_groups=mesh['grp'=2,'sp_0'=16,'sp_1'=2,'tp'=4] {'sp_1'}, dimensions={0}, use_global_device_ids=true | all-gather | bytes 24 | tf_op jit(solution)/shard_map/all_gather | solution.py:30
  30.1 0.9 bitcast_convert_fusion
  31.0 0.1 rev.18
  31.1 0.9 copy.84
  32.1 0.2 reverse.3
  32.3 0.2 convolution_add_fusion.1
  32.4 2.0 all-gather.1
  34.5 0.7 bitcast_add_fusion
  35.2 0.1 all-gather.12.cloned.1.call-update
  35.3 0.1 all-gather.10.cloned.1.call-start
  35.4 0.3 reduce_window_sum.17
  35.7 0.2 exponential_reduce_fusion.1
  35.9 1.9 all-gather.2
  37.7 0.2 slice_reduce_fusion.1
  37.9 0.1 bitcast_exponential_fusion.1
  38.0 0.2 convolution_add_fusion
  38.2 2.0 all-gather
  40.2 0.7 bitcast_add_fusion.2
  41.0 0.1 all-gather.14.cloned.1.call-start
  41.1 0.9 pad_maximum_fusion.2
  42.0 0.1 all-gather.14.cloned.1.call-update
  42.1 0.1 copy.54
  42.3 0.1 rev.16
  42.4 23.7 %all-gather.3 = f32[16,1,2]{2,1,0:T(1,128)S(1)} all-gather(f32[1,1,2]{2,1,0:T(1,128)S(1)} %get-tuple-element.78), channel_id=1, replica_groups=mesh['grp'=2,'sp_0'=16,'sp_1'=2,'tp'=4] {'sp_0'}, dimensions={0}, use_global_device_ids=true | all-gather | bytes 136 | tf_op jit(solution)/shard_map/all_gather | solution.py:30
  66.0 20.6 %all-gather.5 = f32[16,1,2]{2,1,0:T(1,128)S(1)} all-gather(f32[1,1,2]{2,1,0:T(1,128)S(1)} %get-tuple-element.84), channel_id=1, replica_groups=mesh['grp'=2,'sp_0'=16,'sp_1'=2,'tp'=4] {'sp_0'}, dimensions={0}, use_global_device_ids=true | all-gather | bytes 136 | tf_op jit(solution)/shard_map/all_gather | solution.py:30
  86.7 0.2 fusion.197
  87.0 0.2 fusion.194
  87.2 5.4 %all-gather.12.cloned.1.call-done = f32[16,2,128,128]{3,2,1,0:T(8,128)} async-done(((f32[1,2,128,128]{3,2,1,0:T(8,128)}), f32[16,2,128,128]{3,2,1,0:T(8,128)}) %all-gather.12.cloned.1.call-update) | async-done | bytes 2097168 | tf_op jit(solution)/shard_map/all_gather | solution.py:30
  92.6 2.1 convolution_bitcast_fusion
  94.7 0.4 fusion.15
  95.1 0.1 rev.19
  95.2 0.1 reduce_sum.65
  95.3 0.2 multiply_reduce_fusion
  95.5 0.1 subtract_multiply_fusion
  95.7 0.1 copy.73
  95.8 65.3 %all-gather.10.cloned.1.call-done = f32[16,2,128,128]{3,2,1,0:T(8,128)} async-done(((f32[1,2,128,128]{3,2,1,0:T(8,128)}), f32[16,2,128,128]{3,2,1,0:T(8,128)}) %all-gather.10.cloned.1.call-update) | async-done | bytes 2097168 | tf_op jit(solution)/shard_map/all_gather | solution.py:30
  161.0 2.1 convolution_bitcast_fusion.3
  163.2 0.4 fusion.322
  163.7 0.1 fusion.188
  163.8 1.1 convolution_convert_fusion
  165.0 4.0 %all-to-all-start = ((bf16[4,32,2048]{2,1,0:T(8,128)(2,1)}), bf16[4,32,2048]{2,1,0:T(8,128)(2,1)S(1)}, u32[]{:S(2)}, u32[]{:S(2)}) async-start(bf16[4,32,2048]{2,1,0:T(8,128)(2,1)} %bitcast.98), calls=%async_computation | async-start | bytes 1048576 | tf_op jit(solution)/shard_map/all_to_all | solution.py:57
  169.0 6.9 %all-to-all-done = bf16[4,32,2048]{2,1,0:T(8,128)(2,1)S(1)} async-done(((bf16[4,32,2048]{2,1,0:T(8,128)(2,1)}), bf16[4,32,2048]{2,1,0:T(8,128)(2,1)S(1)}, u32[]{:S(2)}, u32[]{:S(2)}) %all-to-all-start) | async-done | bytes 524320 | tf_op jit(solution)/shard_map/all_to_all | solution.py:57
  175.9 0.1 convert_reduce_fusion.1
  176.0 0.9 add_convert_fusion
  176.9 0.1 fusion.23
  177.1 0.1 fusion.25
  177.2 12.1 %all_to_all.15 = bf16[4,32,2048]{2,1,0:T(8,128)(2,1)S(1)} all-to-all(bf16[4,32,2048]{2,1,0:T(8,128)(2,1)S(1)} %broadcast_in_dim.28), channel_id=1, replica_groups=mesh['grp'=2,'sp_0'=16,'sp_1'=2,'tp'=4] {'tp'}, dimensions={0} | all-to-all | bytes 1048576 | tf_op jit(solution)/shard_map/all_to_all | solution.py:63
  189.4 88.3 %all-gather.14.cloned.1.call-done = bf16[2048,4224]{1,0:T(8,128)(2,1)} async-done(((bf16[64,4224]{1,0:T(8,128)(2,1)}), bf16[2048,4224]{1,0:T(8,128)(2,1)}) %all-gather.14.cloned.1.call-update) | async-done | bytes 17301520 | tf_op jit(solution)/shard_map/all_gather | solution.py:46
  277.7 6.0 %fusion.4 = bf16[128,2816]{1,0:T(8,128)(2,1)S(1)} fusion(bf16[128,2048]{1,0:T(8,128)(2,1)S(1)} %bitcast.488, bf16[2048,4224]{1,0:T(8,128)(2,1)} %all-gather.14.cloned.1.call-done), kind=kOutput, calls=%fused_computation.4 | convolution fusion | flops 1476755456 | bytes 12779520 | tf_op jit(solution)/shard_map/dot_general | solution.py:202
  283.8 2.0 collective-permute-start
  285.7 2.4 collective-permute-start.1
  288.2 0.1 convert_reduce_fusion.3
  288.3 2.5 collective-permute-done.1
  290.7 0.5 multiply_add_fusion
  291.2 4.6 %fusion.7 = bf16[128,2048]{1,0:T(8,128)(2,1)S(1)} fusion(bf16[2048,4224]{1,0:T(8,128)(2,1)} %all-gather.14.cloned.1.call-done, f32[128,2816]{1,0:T(8,128)S(1)} %multiply_add_fusion), kind=kOutput, calls=%fused_computation.5 | convolution fusion | flops 739540992 | bytes 7733248 | tf_op jit(solution)/shard_map/dot_general | solution.py:216
  295.9 12.8 %all_to_all.16 = bf16[4,32,2048]{2,1,0:T(8,128)(2,1)S(1)} all-to-all(bf16[4,32,2048]{2,1,0:T(8,128)(2,1)S(1)} %bitcast.489), channel_id=1, replica_groups=mesh['grp'=2,'sp_0'=16,'sp_1'=2,'tp'=4] {'tp'}, dimensions={0} | all-to-all | bytes 1048576 | tf_op jit(solution)/shard_map/all_to_all | solution.py:57
  308.7 0.1 convert_reduce_fusion
  308.8 0.7 fusion.26
  (46 shorter events, 0.3 us)
Async XLA Ops:
  6.5 157.3 %copy-start = (bf16[256,2048]{1,0:T(8,128)(2,1)S(1)}, bf16[256,2048]{1,0:T(8,128)(2,1)}, u32[]{:S(2)}) copy-start(bf16[256,2048]{1,0:T(8,128)(2,1)} %param.20) | copy-start | bytes 3145732
  6.6 31.4 %copy-start.2 = (bf16[128,256]{1,0:T(8,128)(2,1)S(1)}, bf16[128,256]{1,0:T(8,128)(2,1)}, u32[]{:S(2)}) copy-start(bf16[128,256]{1,0:T(8,128)(2,1)} %param.16) | copy-start | bytes 196612
  6.6 86.0 %all-gather.12.cloned.1.call-start = ((), (), s32[]{:S(2)}) async-start(), calls=%async_computation.4 | async-start | bytes 2228224 | tf_op jit(solution)/shard_map/all_gather | solution.py:30
  32.1 9.1 %copy-start.3 = (bf16[64,1408]{1,0:T(8,128)(2,1)S(1)}, bf16[64,1408]{1,0:T(8,128)(2,1)}, u32[]{:S(2)}) copy-start(bf16[64,1408]{1,0:T(8,128)(2,1)} %param.25) | copy-start | bytes 540676
  32.1 9.0 %copy-start.4 = (bf16[64,1408]{1,0:T(8,128)(2,1)S(1)}, bf16[64,1408]{1,0:T(8,128)(2,1)}, u32[]{:S(2)}) copy-start(bf16[64,1408]{1,0:T(8,128)(2,1)} %param.24) | copy-start | bytes 540676
  32.1 9.0 %copy-start.5 = (bf16[64,1408]{1,0:T(8,128)(2,1)S(1)}, bf16[64,1408]{1,0:T(8,128)(2,1)}, u32[]{:S(2)}) copy-start(bf16[64,1408]{1,0:T(8,128)(2,1)} %param.23) | copy-start | bytes 540676
  35.3 125.8 %all-gather.10.cloned.1.call-start = ((), (), s32[]{:S(2)}) async-start(), calls=%async_computation.3 | async-start | bytes 2228224 | tf_op jit(solution)/shard_map/all_gather | solution.py:30
  38.0 4.1 %copy-start.6 = (bf16[128,256]{1,0:T(8,128)(2,1)S(1)}, bf16[128,256]{1,0:T(8,128)(2,1)}, u32[]{:S(2)}) copy-start(bf16[128,256]{1,0:T(8,128)(2,1)} %param.17) | copy-start | bytes 196612
  38.2 4.1 %copy-start.1 = (bf16[128,256]{1,0:T(8,128)(2,1)S(1)}, bf16[128,256]{1,0:T(8,128)(2,1)}, u32[]{:S(2)}) copy-start(bf16[128,256]{1,0:T(8,128)(2,1)} %param.14) | copy-start | bytes 196612
  40.2 46.5 %copy-start.10 = (f32[2,256]{1,0:T(2,128)S(1)}, f32[2,256]{1,0:T(2,128)}, u32[]{:S(2)}) copy-start(f32[2,256]{1,0:T(2,128)} %param.19) | copy-start | bytes 6148
  41.0 236.7 %all-gather.14.cloned.1.call-start = ((), (), s32[]{:S(2)}) async-start(), calls=%async_computation.5 | async-start | bytes 17842176 | tf_op jit(solution)/shard_map/all_gather | solution.py:46
  163.8 5.1 %copy-start.9 = (bf16[2048]{0:T(1024)(128)(2,1)S(1)}, bf16[2048]{0:T(1024)(128)(2,1)}, u32[]{:S(2)}) copy-start(bf16[2048]{0:T(1024)(128)(2,1)} %param.22) | copy-start | bytes 12292
  165.0 10.9 %all-to-all-start = ((bf16[4,32,2048]{2,1,0:T(8,128)(2,1)}), bf16[4,32,2048]{2,1,0:T(8,128)(2,1)S(1)}, u32[]{:S(2)}, u32[]{:S(2)}) async-start(bf16[4,32,2048]{2,1,0:T(8,128)(2,1)} %bitcast.98), calls=%async_computation | async-start | bytes 1048576 | tf_op jit(solution)/shard_map/all_to_all | solution.py:57
  277.7 10.4 %copy-start.7 = (bf16[3,1408]{1,0:T(4,128)(2,1)S(1)}, bf16[3,1408]{1,0:T(4,128)(2,1)}, u32[]{:S(2)}) copy-start(bf16[3,1408]{1,0:T(4,128)(2,1)} %param.27) | copy-start | bytes 25348
  277.7 10.4 %copy-start.8 = (bf16[3,1408]{1,0:T(4,128)(2,1)S(1)}, bf16[3,1408]{1,0:T(4,128)(2,1)}, u32[]{:S(2)}) copy-start(bf16[3,1408]{1,0:T(4,128)(2,1)} %param.26) | copy-start | bytes 25348
  283.8 4.5 %collective-permute-start = (bf16[1,2816]{1,0:T(2,128)(2,1)S(1)}, bf16[1,2816]{1,0:T(2,128)(2,1)S(1)}, u32[]{:S(2)}, u32[]{:S(2)}) collective-permute-start(bf16[1,2816]{1,0:T(2,128)(2,1)S(1)} %get-tuple-element.31), channel_id=1, source_target_pairs={{0,4},{4,8},{8,12},{12,16},{16,20},{20,24},{24,28},{28,32},{32,36}... | collective-permute-start | bytes 16904 | tf_op jit(solution)/shard_map/ppermute | solution.py:86
  285.7 5.0 %collective-permute-start.1 = (bf16[1,2816]{1,0:T(2,128)(2,1)S(1)}, bf16[1,2816]{1,0:T(2,128)(2,1)S(1)}, u32[]{:S(2)}, u32[]{:S(2)}) collective-permute-start(bf16[1,2816]{1,0:T(2,128)(2,1)S(1)} %get-tuple-element.32), channel_id=1, source_target_pairs={{4,0},{8,4},{12,8},{16,12},{20,16},{24,20},{28,24},{32,28},{36,32}... | collective-permute-start | bytes 16904 | tf_op jit(solution)/shard_map/ppermute | solution.py:87
Sparse Core Ops, SparseCore 0:
  35.4 57.1 all-gather.11
  94.4 66.6 all-gather.9
  162.9 114.7 all-gather.13
where the time goes:
time: 317 us; the launch traced here: 316 us
  waiting for transfers between devices  169 us (53%)
  blocking collectives  97.2 us (31%)
  matrix products  17.6 us (6%)
  between operations  13.6 us (4%)
  starting transfers between devices  8.5 us (3%)
  other arithmetic  6.44 us (2%)
  local copies, waits for them, and re-layouts  4.2 us (1%)
    all_gather x1, waiting for transfers between devices, sent_together(): lax.all_gather(both, axis, axis=dim, tiled=True)  88.3 us
    all_gather x6, blocking collectives, entering_2(): pieces = jax.tree.map(lambda part: lax.all_gather(part, axis), running)  72.2 us
    all_gather x2, waiting for transfers between devices, entering_2(): pieces = jax.tree.map(lambda part: lax.all_gather(part, axis), running)  70.7 us
    all_to_all x1, blocking collectives, summed_on_arrival(): lax.all_to_all(parts, axis, split_axis=0, concat_axis=0, tiled=True)  12.8 us
    all_to_all x1, blocking collectives, sent_to_all(): lax.all_to_all(jnp.broadcast_to(shard[None], (length, *shard.shape)), axi...  12.1 us
    all_to_all x1, waiting for transfers between devices, summed_on_arrival(): lax.all_to_all(parts, axis, split_axis=0, concat_axis=0, tiled=True)  6.93 us
  transfers between devices with their start and end apart: 6, of which 5 were waited for; matrix products, arithmetic and copies ran while one was open for 4% of the time, Pallas kernels for 0%

commit v1 on v0

v1 whole, which is shorter than its diff:
```python
import math

import jax
import jax.numpy as jnp
from jax import lax
from jax.experimental import pallas as pl
from jax.experimental.pallas import tpu as pltpu
from jax.sharding import Mesh
from jax.sharding import PartitionSpec as P

HEAD = 128
LANES = 128
SP = ("z", "c")
ROWS = ("pg", "pr", "z", "c")
PEERS = ("pr", "tp")

GROUP_EPS = 1e-05
NORM_EPS = 1e-06

F32 = jnp.float32
BF16 = jnp.bfloat16
VMEM = pl.BlockSpec(memory_space=pltpu.VMEM)


def call(body, outs, *args):
    return pl.pallas_call(
        body,
        out_shape=outs,
        in_specs=[VMEM] * len(args),
        out_specs=jax.tree.map(lambda _: VMEM, outs),
    )(*args)


def shaped(shape, dtype):
    return jax.ShapeDtypeStruct(shape, dtype)


def dot(a, b, dims=((1,), (0,))):
    return lax.dot_general(a, b, (dims, ((), ())), preferred_element_type=F32)


def split_columns(pair, width):
    tiles = width // LANES
    share = -(-tiles // pair)
    step = (tiles - share) // (pair - 1) if pair > 1 else 0
    return share * LANES, step * LANES


def pick_weights(pair, gate_ref, up_ref, down_ref, out_ref):
    cols, step = split_columns(pair, gate_ref.shape[1])
    start = pl.multiple_of(lax.axis_index("pr") * step, LANES)
    for i, ref in enumerate((gate_ref, up_ref, down_ref)):
        out_ref[:, i * cols : (i + 1) * cols] = ref[:, pl.ds(start, cols)]


def local_retention(q_ref, k_ref, v_ref, rate_ref, inner_ref, query_ref, keep_ref, send_ref):
    n, width = q_ref.shape
    heads = width // HEAD
    row = lax.broadcasted_iota(jnp.int32, (n, n), 0)
    col = lax.broadcasted_iota(jnp.int32, (n, n), 1)
    scale = HEAD ** (-0.5)
    first = lax.axis_index("c") == 0
    for h in range(heads):
        cut = slice(h * HEAD, (h + 1) * HEAD)
        q, k, v = q_ref[:, cut], k_ref[:, cut], v_ref[:, cut]
        scores = dot(q, k, ((1,), (1,))) * scale
        states, decays = [], []
        for way in range(2):
            rate = rate_ref[way, h : h + 1, :]
            rate_col = jnp.sum(jnp.where(row == col, rate, 0.0), axis=1, keepdims=True)
            seen = col <= row if way == 0 else col >= row
            seen_by = row <= col if way == 0 else row >= col
            total_col = jnp.sum(jnp.where(seen, rate, 0.0), axis=1, keepdims=True)
            total_row = jnp.sum(jnp.where(seen_by, rate_col, 0.0), axis=0, keepdims=True)
            whole = jnp.sum(rate, axis=1, keepdims=True)
            mask = jnp.where(seen, jnp.exp(jnp.minimum(total_col - total_row, 0.0)), 0.0)
            inner_ref[way, :, cut] = dot((scores * mask).astype(BF16), v)
            query_ref[way, :, cut] = (q.astype(F32) * jnp.exp(total_col)).astype(BF16)
            weight = jnp.exp(whole - total_col) * scale
            states.append(dot((k.astype(F32) * weight).astype(BF16), v, ((0,), (0,))))
            decays.append(jnp.broadcast_to(jnp.exp(whole), (1, HEAD)))
        rows = slice(h * HEAD, (h + 1) * HEAD)
        keep_ref[rows, :] = jnp.where(first, states[0], states[1])
        send_ref[rows, :] = jnp.where(first, states[1], states[0])
        mark = slice(heads * HEAD + h, heads * HEAD + h + 1)
        keep_ref[mark, :] = jnp.where(first, decays[0], decays[1])
        send_ref[mark, :] = jnp.where(first, decays[1], decays[0])


def pack_states(keep_ref, got_ref, out_ref):
    pieces = out_ref.shape[0]
    heads = keep_ref.shape[0] // HEAD
    rows = HEAD // pieces
    marks = []
    for h in range(heads):
        at = heads * HEAD + h
        a = keep_ref[at : at + 1, :] * got_ref[at : at + 1, :]
        high = a.astype(BF16).astype(F32)
        middle = (a - high).astype(BF16).astype(F32)
        low = a - high - middle
        marks += [high, middle, low]
    used = heads * rows
    marks.append(jnp.zeros((out_ref.shape[1] - used - len(marks), LANES), F32))
    marks = jnp.concatenate(marks, axis=0).astype(BF16)
    for z in range(pieces):
        parts = []
        for h in range(heads):
            at = heads * HEAD + h
            cut = slice(h * HEAD + z * rows, h * HEAD + (z + 1) * rows)
            parts.append(keep_ref[cut, :] * got_ref[at : at + 1, :] + got_ref[cut, :])
        out_ref[z, 0:used, :] = jnp.concatenate(parts, axis=0).astype(BF16)
        out_ref[z, used:, :] = marks


def scan_states(in_ref, out_ref):
    pieces, used, _ = out_ref.shape
    first = lax.axis_index("c") == 0
    half = used // 2
    state = jnp.zeros((used, LANES), F32)
    for t in range(pieces):
        j = jnp.where(first, t, pieces - 1 - t)
        part = in_ref[j].astype(F32)
        out_ref[j] = state.astype(BF16)
        decay = [
            jnp.sum(part[used + 3 * h : used + 3 * h + 3, :], axis=0, keepdims=True)
            for h in range(2)
        ]
        decay = jnp.concatenate([jnp.broadcast_to(d, (half, LANES)) for d in decay], axis=0)
        state = state * decay + part[:used, :]


def spread_states(in_ref, keep_ref, own_ref, send_ref):
    pieces, used, _ = in_ref.shape
    heads = own_ref.shape[0] // HEAD
    rows = used // heads
    for h in range(heads):
        at = heads * HEAD + h
        state = jnp.concatenate(
            [in_ref[z].astype(F32)[h * rows : (h + 1) * rows, :] for z in range(pieces)], axis=0
        )
        cut = slice(h * HEAD, (h + 1) * HEAD)
        own_ref[cut, :] = state.astype(BF16)
        send_ref[cut, :] = (state * keep_ref[at : at + 1, :] + keep_ref[cut, :]).astype(BF16)


def group_norm(values):
    centre = values - jnp.mean(values, axis=1, keepdims=True)
    spread = jnp.mean(centre * centre, axis=1, keepdims=True)
    return centre * lax.rsqrt(spread + GROUP_EPS)


def mix(inner_ref, query_ref, own_ref, got_ref, gate_ref, gain_ref, weight_ref, out_ref):
    heads = gate_ref.shape[1] // HEAD
    first = lax.axis_index("c") == 0
    mixed = []
    for h in range(heads):
        cut = slice(h * HEAD, (h + 1) * HEAD)
        own, got = own_ref[cut, :], got_ref[cut, :]
        combined = 0.0
        for way in range(2):
            state = jnp.where(first, own, got) if way == 0 else jnp.where(first, got, own)
            values = inner_ref[way, :, cut] + dot(query_ref[way, :, cut], state)
            combined = combined + group_norm(values) * gain_ref[way : way + 1, cut]
        gate = gate_ref[:, cut].astype(F32)
        mixed.append((gate / (1.0 + jnp.exp(-gate)) * combined).astype(BF16))
    mixed = jnp.concatenate(mixed, axis=1)
    attended = dot(mixed, weight_ref[...]).astype(BF16)
    parts, rows, _ = out_ref.shape
    for p in range(parts):
        out_ref[p] = attended[p * rows : (p + 1) * rows, :]


def finish_middle(in_ref, residual_ref, gain_ref, middle_ref, out_ref):
    rows = middle_ref.shape[0]
    start = pl.multiple_of(lax.axis_index("tp") * rows, rows)
    attended = jnp.sum(in_ref[...].astype(F32), axis=0)
    middle = (residual_ref[pl.ds(start, rows), :].astype(F32) + attended).astype(BF16)
    middle_ref[...] = middle
    values = middle.astype(F32)
    scale = lax.rsqrt(jnp.mean(values * values, axis=1, keepdims=True) + NORM_EPS)
    normed = (values * scale * gain_ref[...].astype(F32)).astype(BF16)
    for p in range(out_ref.shape[0]):
        out_ref[p] = normed


def convolved(pre, halo, taps, pair):
    n = pre.shape[0] // pair
    row = lax.broadcasted_iota(jnp.int32, (n, pre.shape[1]), 0)
    spans = []
    for s in range(pair):
        x = pre[s * n : (s + 1) * n, :]
        before = jnp.where(row == 0, halo[s : s + 1, :], pltpu.roll(x, 1, 0))
        after = jnp.where(row == n - 1, halo[pair + s : pair + s + 1, :], pltpu.roll(x, n - 1, 0))
        spans.append(taps[0:1] * before + taps[1:2] * x + taps[2:3] * after)
    return jnp.concatenate(spans, axis=0)


def feed_forward(
    pair, x_ref, halo_ref, gate_ref, up_ref, down_ref, gt_ref, ut_ref, out_ref, acc_ref
):
    j = pl.program_id(0)
    block = gate_ref.shape[1]
    cols, step = split_columns(pair, gt_ref.shape[1])
    member = lax.axis_index("pr")
    at = pl.multiple_of(member * step + j * block, LANES)
    column = at + lax.broadcasted_iota(jnp.int32, (1, block), 1)
    x, halo = x_ref[...], halo_ref[...]

    def branch(weight, taps):
        pre = dot(x, weight).astype(BF16).astype(F32)
        edge = dot(halo, weight).astype(BF16).astype(F32)
        return convolved(pre, edge, taps, pair)

    gate = branch(gate_ref[...], gt_ref[:, pl.ds(at, block)].astype(F32))
    taps = jnp.where(column >= member * cols, ut_ref[:, pl.ds(at, block)].astype(F32), 0.0)
    up = branch(up_ref[...], taps)
    hidden = (gate / (1.0 + jnp.exp(-gate)) * up).astype(BF16)
    part = dot(hidden, down_ref[...], ((1,), (1,)))

    @pl.when(j == 0)
    def _():
        acc_ref[...] = part

    @pl.when(j > 0)
    def _():
        acc_ref[...] += part

    @pl.when(j == pl.num_programs(0) - 1)
    def _():
        parts, rows, _ = out_ref.shape
        for p in range(parts):
            out_ref[p] = acc_ref[p * rows : (p + 1) * rows, :].astype(BF16)


def run_feed_forward(pair, peers, normed, halo, gathered, gate_taps, up_taps):
    depth, columns = gathered.shape
    cols = columns // 3
    block = 256
    steps = cols // block
    whole = lambda a: pl.BlockSpec(a.shape, lambda j: (0,) * a.ndim)
    piece = lambda i: pl.BlockSpec((depth, block), lambda j, i=i: (0, i * steps + j))
    rows = normed.shape[0]
    return pl.pallas_call(
        lambda *refs: feed_forward(pair, *refs),
        grid=(steps,),
        out_shape=shaped((peers, rows // peers, depth), BF16),
        in_specs=[whole(normed), whole(halo), piece(0), piece(1), piece(2)]
        + [whole(gate_taps), whole(up_taps)],
        out_specs=pl.BlockSpec((peers, rows // peers, depth), lambda j: (0, 0, 0)),
        scratch_shapes=[pltpu.VMEM((rows, depth), F32)],
    )(normed, halo, gathered, gathered, gathered, gate_taps, up_taps)


def across(x, axes):
    return lax.all_to_all(x, axes, 0, 0, tiled=True)


def shards(
    query_rows,
    key_rows,
    value_rows,
    gate_rows,
    log_decay,
    head_gain,
    out_weight,
    residual,
    norm_gain,
    gate_weight,
    up_weight,
    down_weight,
    gate_taps,
    up_taps,
):
    pair, chips, tp = lax.axis_size("pr"), lax.axis_size("z"), lax.axis_size("tp")
    peers = pair * tp
    rows, width = query_rows.shape
    depth = residual.shape[1]
    heads = width // HEAD
    cols, _ = split_columns(pair, gate_weight.shape[1])

    picked = call(
        lambda *refs: pick_weights(pair, *refs),
        shaped((gate_weight.shape[0], 3 * cols), BF16),
        gate_weight,
        up_weight,
        down_weight,
    )
    gathered = lax.all_gather(picked, SP, axis=0, tiled=True)

    marked = shaped((heads * HEAD + 8, HEAD), F32)
    inner, query, keep, send = call(
        local_retention,
        (shaped((2, rows, width), F32), shaped((2, rows, width), BF16), marked, marked),
        query_rows,
        key_rows,
        value_rows,
        log_decay,
    )
    swap = [(0, 1), (1, 0)]
    got = lax.ppermute(send, "c", swap)
    used = heads * HEAD // chips
    message = call(pack_states, shaped((chips, used + 16, HEAD), BF16), keep, got)
    prefix = call(scan_states, shaped((chips, used, HEAD), BF16), across(message, "z"))
    state = shaped((heads * HEAD, HEAD), BF16)
    own, other = call(spread_states, (state, state), across(prefix, "z"), keep)
    entering = lax.ppermute(other, "c", swap)
    attended = call(
        mix,
        shaped((tp, rows // tp, depth), BF16),
        inner,
        query,
        own,
        entering,
        gate_rows,
        head_gain,
        out_weight,
    )
    middle, copies = call(
        finish_middle,
        (shaped((rows // tp, depth), BF16), shaped((peers, rows // tp, depth), BF16)),
        across(attended, "tp"),
        residual,
        norm_gain.reshape(1, depth),
    )
    normed = across(copies, PEERS).reshape(pair, rows, depth)
    size = lax.axis_size("z") * lax.axis_size("c")
    onward = [(i, i + 1) for i in range(size - 1)]
    back = [(j, i) for i, j in onward]
    before = lax.ppermute(normed[:, rows - 1], SP, onward)
    after = lax.ppermute(normed[:, 0], SP, back)
    fill = jnp.zeros((16 - 2 * pair, depth), BF16)
    halo = jnp.concatenate([before, after, fill], axis=0)
    parts = run_feed_forward(
        pair, peers, normed.reshape(pair * rows, depth), halo, gathered, gate_taps, up_taps
    )
    summed = across(parts, PEERS).astype(F32).sum(axis=0)
    return (middle.astype(F32) + summed).astype(BF16)


def solution(mesh):
    groups, tp = mesh.shape["grp"], mesh.shape["tp"]
    pair = math.gcd(groups, 2)
    split = Mesh(
        mesh.devices.reshape(groups // pair, pair, mesh.shape["sp"] // 2, 2, tp),
        ("pg", "pr", "z", "c", "tp"),
    )
    placed = (
        P(ROWS, "tp"),
        P(ROWS, "tp"),
        P(ROWS, "tp"),
        P(ROWS, "tp"),
        P(None, "tp", ROWS),
        P(None, "tp"),
        P("tp", None),
        P(ROWS, None),
        P(),
        P(SP, "tp"),
        P(SP, "tp"),
        P(SP, "tp"),
        P(None, "tp"),
        P(None, "tp"),
    )
    return jax.shard_map(
        shards, mesh=split, in_specs=placed, out_specs=P((*ROWS, "tp"), None), check_vma=False
    )
```

time: 317 us -> 160 us (0.50)
  waiting for transfers between devices: 169 us -> 10.7 us
  starting transfers between devices: 8.5 us -> 35.4 us
  blocking collectives: 97.2 us -> 71.6 us
  Pallas kernels: 0 us -> 23.1 us
  matrix products: 17.6 us -> 0 us
  other arithmetic: 6.44 us -> 1.51 us
    all_gather x3 -> x1, waiting for transfers between devices: 159 us -> 0.01 us  [shards(): gathered = lax.all_gather(picked, SP, axis=0, tiled=True)]
    all_gather x6 -> x0, blocking collectives: 72.2 us -> none  [entering_2(): pieces = jax.tree.map(lambda part: lax.all_gather(part, axis), running)]
    all_to_all x2 -> x4, blocking collectives: 25 us -> 71.6 us  [across(): return lax.all_to_all(x, axes, 0, 0, tiled=True)]
    ppermute x2 -> x4, starting transfers between devices: 4.38 us -> 31.1 us  [the longest x1 20.4 us: shards(): got = lax.ppermute(send, 'c', swap)]
    pallas_call x0 -> x8, Pallas kernels: none -> 23.1 us  [the longest x7 14.3 us: call(): pl.pallas_call(body, out_shape=outs, in_specs=[VMEM] * len(args), out_spe...]
    dot_general x11 -> x0, matrix products: 17.6 us -> none  [the longest x1 5.98 us: shards(): jnp.dot(gathered_copies(normed, 'tp', 0), pair_full, preferred_element_ty...]
  transfers between devices with their start and end apart: 6 -> 6, of which waited for: 5 -> 4; matrix products, arithmetic and copies ran while one was open for 4% -> 1% of each run, Pallas kernels for 0% -> 8%
where the time goes in v1:
time: 160 us; the launch traced here: 159 us
  blocking collectives  71.6 us (45%)
  starting transfers between devices  35.4 us (22%)
  Pallas kernels  23.1 us (14%)
  between operations  13.5 us (8%)
  waiting for transfers between devices  10.7 us (7%)
  local copies, waits for them, and re-layouts  3.51 us (2%)
    all_to_all x4, blocking collectives, across(): return lax.all_to_all(x, axes, 0, 0, tiled=True)  71.6 us
    ppermute x1, starting transfers between devices, shards(): got = lax.ppermute(send, 'c', swap)  20.4 us
    pallas_call x7, Pallas kernels, call(): pl.pallas_call(body, out_shape=outs, in_specs=[VMEM] * len(args), out_spe...  14.3 us
    pallas_call x1, Pallas kernels, run_feed_forward(): pl.pallas_call(lambda *refs: feed_forward(pair, *refs), grid=(steps,), ou...  8.78 us
    all_to_all x1, waiting for transfers between devices, across(): return lax.all_to_all(x, axes, 0, 0, tiled=True)  7.64 us
    ppermute x1, starting transfers between devices, shards(): after = lax.ppermute(normed[:, 0], SP, back)  5.53 us
    all_to_all x1, starting transfers between devices, across(): return lax.all_to_all(x, axes, 0, 0, tiled=True)  4.26 us
  transfers between devices with their start and end apart: 6, of which 4 were waited for; matrix products, arithmetic and copies ran while one was open for 1% of the time, Pallas kernels for 8%

profile of v1, /device:TPU:33, one launch (start us, length us, event | category | flops | bytes accessed | tf_op | source)
XLA Modules:
  0.0 159.3 jit_solution(14440589199043664785)
XLA Ops:
  6.5 0.0 all-gather.2.cloned.1.call-start
  6.6 1.8 %shard_map.142 = bf16[64,2304]{1,0:T(8,128)(2,1)} custom-call(bf16[64,1408]{1,0:T(8,128)(2,1)} %refs_0_.1, bf16[64,1408]{1,0:T(8,128)(2,1)} %refs_1_.1, bf16[64,1408]{1,0:T(8,128)(2,1)} %refs_2_.1), custom_call_target="tpu_custom_call" | custom-call | tf_op jit(solution)/shard_map/pallas_call | solution.py:26
  8.4 0.1 all-gather.2.cloned.1.call-update
  8.4 2.2 %shard_map.136 = (f32[2,128,256]{2,1,0:T(8,128)}, bf16[2,128,256]{2,1,0:T(8,128)(2,1)}, f32[264,128]{1,0:T(8,128)}, f32[264,128]{1,0:T(8,128)}) custom-call(bf16[128,256]{1,0:T(8,128)(2,1)} %q_ref.1, bf16[128,256]{1,0:T(8,128)(2,1)} %k_ref.1, bf16[128,256]{1,0:T(8,128)(2,1)} %v_ref.1, f32[2,2,128]{2,1,0:T(2,128)} %rate_ref.1), custom_call_target="tpu_custom_call" | custom-call | tf_op jit(solution)/shard_map/pallas_call | solution.py:26
  10.6 20.4 %collective-permute-start = (f32[264,128]{1,0:T(8,128)}, f32[264,128]{1,0:T(8,128)S(1)}, u32[]{:S(2)}, u32[]{:S(2)}) collective-permute-start(f32[264,128]{1,0:T(8,128)} %get-tuple-element.16), channel_id=1, source_target_pairs={{0,4},{4,0},{1,5},{5,1},{2,6},{6,2},{3,7},{7,3},{8,12},{12,8},{9,1... | collective-permute-start | bytes 405512 | tf_op jit(solution)/shard_map/ppermute | solution.py:300
  31.1 1.2 collective-permute-done.got_ref
  32.3 0.0 copy-start.2
  32.3 0.7 copy-done.2
  32.9 1.6 %shard_map.137 = bf16[16,32,128]{2,1,0:T(8,128)(2,1)} custom-call(f32[264,128]{1,0:T(8,128)} %get-tuple-element.15.keep_ref, f32[264,128]{1,0:T(8,128)} %copy-done.2), custom_call_target="tpu_custom_call" | custom-call | tf_op jit(solution)/shard_map/pallas_call | solution.py:26
  34.6 17.4 %all_to_all.25.in_ref = bf16[16,32,128]{2,1,0:T(8,128)(2,1)} all-to-all(bf16[16,32,128]{2,1,0:T(8,128)(2,1)} %shard_map.137), channel_id=1, replica_groups=mesh['pg'=1,'pr'=2,'z'=16,'c'=2,'tp'=4] {'z'}, dimensions={0} | all-to-all | bytes 262144 | tf_op jit(solution)/shard_map/all_to_all | solution.py:255
  51.9 1.6 shard_map.138
  53.5 19.1 %all_to_all.26.in_ref = bf16[16,16,128]{2,1,0:T(8,128)(2,1)} all-to-all(bf16[16,16,128]{2,1,0:T(8,128)(2,1)} %shard_map.138), channel_id=1, replica_groups=mesh['pg'=1,'pr'=2,'z'=16,'c'=2,'tp'=4] {'z'}, dimensions={0} | all-to-all | bytes 131072 | tf_op jit(solution)/shard_map/all_to_all | solution.py:255
  72.6 1.6 %shard_map.139 = (bf16[256,128]{1,0:T(8,128)(2,1)}, bf16[256,128]{1,0:T(8,128)(2,1)}) custom-call(bf16[16,16,128]{2,1,0:T(8,128)(2,1)} %all_to_all.26.in_ref, f32[264,128]{1,0:T(8,128)} %get-tuple-element.15.keep_ref), custom_call_target="tpu_custom_call" | custom-call | tf_op jit(solution)/shard_map/pallas_call | solution.py:26
  74.2 2.9 %collective-permute-start.1 = (bf16[256,128]{1,0:T(8,128)(2,1)}, bf16[256,128]{1,0:T(8,128)(2,1)S(1)}, u32[]{:S(2)}, u32[]{:S(2)}) collective-permute-start(bf16[256,128]{1,0:T(8,128)(2,1)} %get-tuple-element.18), channel_id=1, source_target_pairs={{0,4},{4,0},{1,5},{5,1},{2,6},{6,2},{3,7},{7,3},{8,12},{12,8},{9,1... | collective-permute-start | bytes 196616 | tf_op jit(solution)/shard_map/ppermute | solution.py:306
  77.1 1.1 collective-permute-done.1.got_ref
  78.2 0.0 copy-start.4
  78.2 0.6 copy-done.4
  78.8 3.0 %shard_map.140 = bf16[4,32,2048]{2,1,0:T(8,128)(2,1)} custom-call(f32[2,128,256]{2,1,0:T(8,128)} %get-tuple-element.13.inner_ref, bf16[2,128,256]{2,1,0:T(8,128)(2,1)} %get-tuple-element.14.query_ref, bf16[256,128]{1,0:T(8,128)(2,1)} %get-tuple-element.17.own_ref, bf16[256,128]{1,0:T(8,128)(2,1)} %copy-done.4, bf16[128,256]{1,0:T(8,128)(2,1)} %gate_ref.1, ...), custom_call_target="tpu_custom_call" | custom-call | tf_op jit(solution)/shard_map/pallas_call | solution.py:26
  81.8 4.3 %all-to-all-start.2 = ((bf16[4,32,2048]{2,1,0:T(8,128)(2,1)}), bf16[4,32,2048]{2,1,0:T(8,128)(2,1)S(1)}, u32[]{:S(2)}, u32[]{:S(2)}) async-start(bf16[4,32,2048]{2,1,0:T(8,128)(2,1)} %shard_map.140), calls=%async_computation.2 | async-start | bytes 1048576 | tf_op jit(solution)/shard_map/all_to_all | solution.py:255
  86.1 1.3 reshape.6.gain_ref
  87.4 7.6 %all-to-all-done.2.in_ref = bf16[4,32,2048]{2,1,0:T(8,128)(2,1)S(1)} async-done(((bf16[4,32,2048]{2,1,0:T(8,128)(2,1)}), bf16[4,32,2048]{2,1,0:T(8,128)(2,1)S(1)}, u32[]{:S(2)}, u32[]{:S(2)}) %all-to-all-start.2) | async-done | bytes 524320 | tf_op jit(solution)/shard_map/all_to_all | solution.py:255
  95.0 0.0 copy-start.1
  95.0 0.8 copy-done.1
  95.8 2.5 %shard_map.141 = (bf16[32,2048]{1,0:T(8,128)(2,1)}, bf16[8,32,2048]{2,1,0:T(8,128)(2,1)}) custom-call(bf16[4,32,2048]{2,1,0:T(8,128)(2,1)} %copy-done.1, bf16[128,2048]{1,0:T(8,128)(2,1)} %residual_ref.1, bf16[1,2048]{1,0:T(2,128)(2,1)} %reshape.6.gain_ref), custom_call_target="tpu_custom_call" | custom-call | tf_op jit(solution)/shard_map/pallas_call | solution.py:26
  98.3 16.9 %all_to_all.27 = bf16[8,32,2048]{2,1,0:T(8,128)(2,1)S(1)} all-to-all(bf16[8,32,2048]{2,1,0:T(8,128)(2,1)} %get-tuple-element.20), channel_id=1, replica_groups=mesh['pg'=1,'pr'=2,'z'=16,'c'=2,'tp'=4] {'pr','tp'}, dimensions={0} | all-to-all | bytes 2097152 | tf_op jit(solution)/shard_map/all_to_all | solution.py:255
  115.2 0.0 copy-start
  115.3 5.5 %collective-permute-start.3 = (bf16[2,2048]{1,0:T(2,128)(2,1)S(1)}, bf16[2,2048]{1,0:T(2,128)(2,1)S(1)}, u32[]{:S(2)}, u32[]{:S(2)}) collective-permute-start(bf16[2,2048]{1,0:T(2,128)(2,1)S(1)} %bitcast.11), channel_id=1, source_target_pairs={{4,0},{8,4},{12,8},{16,12},{20,16},{24,20},{28,24},{32,28},{36,32}... | collective-permute-start | bytes 24584 | tf_op jit(solution)/shard_map/ppermute | solution.py:330
  120.8 2.3 %collective-permute-start.2 = (bf16[2,2048]{1,0:T(2,128)(2,1)S(1)}, bf16[2,2048]{1,0:T(2,128)(2,1)S(1)}, u32[]{:S(2)}, u32[]{:S(2)}) collective-permute-start(bf16[2,2048]{1,0:T(2,128)(2,1)S(1)} %bitcast.10), channel_id=1, source_target_pairs={{0,4},{4,8},{8,12},{12,16},{16,20},{20,24},{24,28},{28,32},{32,36}... | collective-permute-start | bytes 24584 | tf_op jit(solution)/shard_map/ppermute | solution.py:329
  123.2 0.1 pad.2.clone
  123.3 0.0 collective-permute-done.3
  123.3 0.7 collective-permute-done.2
  123.9 0.7 maximum_maximum_fusion.refs_1_
  124.6 0.0 all-gather.2.cloned.1.call-done.refs_2_.refs_3_.refs_4_
  124.6 0.0 copy-done
  124.6 0.0 copy-start.3
  124.6 8.8 %shard_map.143 = bf16[8,32,2048]{2,1,0:T(8,128)(2,1)} custom-call(bf16[256,2048]{1,0:T(8,128)(2,1)} %bitcast.9, bf16[16,2048]{1,0:T(8,128)(2,1)} %maximum_maximum_fusion.refs_1_, bf16[2048,2304]{1,0:T(8,128)(2,1)} %all-gather.2.cloned.1.call-done.refs_2_.refs_3_.refs_4_, bf16[2048,2304]{1,0:T(8,128)(2,1)} %all-gather.2.cloned.1.call-done.refs_2_.refs_3_.refs_4_, ...), custom_call_target="tpu_custom_call" | custom-call | tf_op jit(solution)/shard_map/pallas_call | solution.py:243
  133.4 18.2 %all_to_all.28 = bf16[8,32,2048]{2,1,0:T(8,128)(2,1)S(1)} all-to-all(bf16[8,32,2048]{2,1,0:T(8,128)(2,1)} %shard_map.143), channel_id=1, replica_groups=mesh['pg'=1,'pr'=2,'z'=16,'c'=2,'tp'=4] {'pr','tp'}, dimensions={0} | all-to-all | bytes 2097152 | tf_op jit(solution)/shard_map/all_to_all | solution.py:255
  151.6 0.1 convert_reduce_fusion
  151.7 0.0 copy-done.3
  151.8 0.7 add_convert_fusion
  (4 shorter events, 0.1 us)
Async XLA Ops:
  6.5 118.1 %all-gather.2.cloned.1.call-start = ((), (), s32[]{:S(2)}) async-start(), calls=%async_computation.5 | async-start | bytes 9732096 | tf_op jit(solution)/shard_map/all_gather | solution.py:288
  10.6 21.6 %collective-permute-start = (f32[264,128]{1,0:T(8,128)}, f32[264,128]{1,0:T(8,128)S(1)}, u32[]{:S(2)}, u32[]{:S(2)}) collective-permute-start(f32[264,128]{1,0:T(8,128)} %get-tuple-element.16), channel_id=1, source_target_pairs={{0,4},{4,0},{1,5},{5,1},{2,6},{6,2},{3,7},{7,3},{8,12},{12,8},{9,1... | collective-permute-start | bytes 405512 | tf_op jit(solution)/shard_map/ppermute | solution.py:300
  32.3 0.7 copy-start.2
  74.2 4.0 %collective-permute-start.1 = (bf16[256,128]{1,0:T(8,128)(2,1)}, bf16[256,128]{1,0:T(8,128)(2,1)S(1)}, u32[]{:S(2)}, u32[]{:S(2)}) collective-permute-start(bf16[256,128]{1,0:T(8,128)(2,1)} %get-tuple-element.18), channel_id=1, source_target_pairs={{0,4},{4,0},{1,5},{5,1},{2,6},{6,2},{3,7},{7,3},{8,12},{12,8},{9,1... | collective-permute-start | bytes 196616 | tf_op jit(solution)/shard_map/ppermute | solution.py:306
  78.2 0.6 copy-start.4
  81.8 13.2 %all-to-all-start.2 = ((bf16[4,32,2048]{2,1,0:T(8,128)(2,1)}), bf16[4,32,2048]{2,1,0:T(8,128)(2,1)S(1)}, u32[]{:S(2)}, u32[]{:S(2)}) async-start(bf16[4,32,2048]{2,1,0:T(8,128)(2,1)} %shard_map.140), calls=%async_computation.2 | async-start | bytes 1048576 | tf_op jit(solution)/shard_map/all_to_all | solution.py:255
  95.0 0.8 copy-start.1
  115.2 9.4 %copy-start = (bf16[8,32,2048]{2,1,0:T(8,128)(2,1)}, bf16[8,32,2048]{2,1,0:T(8,128)(2,1)S(1)}, u32[]{:S(2)}) copy-start(bf16[8,32,2048]{2,1,0:T(8,128)(2,1)S(1)} %all_to_all.27) | copy-start | bytes 3145732
  115.3 8.0 %collective-permute-start.3 = (bf16[2,2048]{1,0:T(2,128)(2,1)S(1)}, bf16[2,2048]{1,0:T(2,128)(2,1)S(1)}, u32[]{:S(2)}, u32[]{:S(2)}) collective-permute-start(bf16[2,2048]{1,0:T(2,128)(2,1)S(1)} %bitcast.11), channel_id=1, source_target_pairs={{4,0},{8,4},{12,8},{16,12},{20,16},{24,20},{28,24},{32,28},{36,32}... | collective-permute-start | bytes 24584 | tf_op jit(solution)/shard_map/ppermute | solution.py:330
  120.8 3.1 %collective-permute-start.2 = (bf16[2,2048]{1,0:T(2,128)(2,1)S(1)}, bf16[2,2048]{1,0:T(2,128)(2,1)S(1)}, u32[]{:S(2)}, u32[]{:S(2)}) collective-permute-start(bf16[2,2048]{1,0:T(2,128)(2,1)S(1)} %bitcast.10), channel_id=1, source_target_pairs={{0,4},{4,8},{8,12},{12,16},{16,20},{20,24},{24,28},{28,32},{32,36}... | collective-permute-start | bytes 24584 | tf_op jit(solution)/shard_map/ppermute | solution.py:329
  124.6 27.1 %copy-start.3 = (bf16[32,2048]{1,0:T(8,128)(2,1)S(1)}, bf16[32,2048]{1,0:T(8,128)(2,1)}, u32[]{:S(2)}) copy-start(bf16[32,2048]{1,0:T(8,128)(2,1)} %get-tuple-element.19) | copy-start | bytes 393220
Sparse Core Ops, SparseCore 0:
  9.2 100.7 all-gather.1

commit v2 on v1

--- a/solution.py
+++ b/solution.py
@@ -20,14 +20,16 @@
 F32 = jnp.float32
 BF16 = jnp.bfloat16
 VMEM = pl.BlockSpec(memory_space=pltpu.VMEM)
-
-
-def call(body, outs, *args):
+HBM = pl.BlockSpec(memory_space=pl.ANY)
+
+
+def call(body, outs, *args, limit=12, **more):
+    spec = {"in_specs": [VMEM] * len(args), "out_specs": jax.tree.map(lambda _: VMEM, outs)}
     return pl.pallas_call(
         body,
         out_shape=outs,
-        in_specs=[VMEM] * len(args),
-        out_specs=jax.tree.map(lambda _: VMEM, outs),
+        compiler_params=pltpu.CompilerParams(vmem_limit_bytes=limit << 20),
+        **{**spec, **more},
     )(*args)
 
 
@@ -46,14 +48,38 @@
     return share * LANES, step * LANES
 
 
-def pick_weights(pair, gate_ref, up_ref, down_ref, out_ref):
+def pick_weights(pair, gate_ref, up_ref, down_ref, out_ref, sems):
     cols, step = split_columns(pair, gate_ref.shape[1])
     start = pl.multiple_of(lax.axis_index("pr") * step, LANES)
-    for i, ref in enumerate((gate_ref, up_ref, down_ref)):
-        out_ref[:, i * cols : (i + 1) * cols] = ref[:, pl.ds(start, cols)]
-
-
-def local_retention(q_ref, k_ref, v_ref, rate_ref, inner_ref, query_ref, keep_ref, send_ref):
+    copies = [
+        pltpu.make_async_copy(
+            ref.at[:, pl.ds(start, cols)], out_ref.at[:, pl.ds(i * cols, cols)], sems.at[i]
+        )
+        for i, ref in enumerate((gate_ref, up_ref, down_ref))
+    ]
+    for copy in copies:
+        copy.start()
+    for copy in copies:
+        copy.wait()
+
+
+def local_retention(
+    q_ref,
+    k_ref,
+    v_ref,
+    rate_ref,
+    weight_ref,
+    inner_ref,
+    query_ref,
+    keep_ref,
+    send_ref,
+    half_ref,
+    sem,
+):
+    half = half_ref.shape[0]
+    start = pl.multiple_of(lax.axis_index("c") * half, half)
+    copy = pltpu.make_async_copy(weight_ref.at[pl.ds(start, half), :], half_ref, sem)
+    copy.start()
     n, width = q_ref.shape
     heads = width // HEAD
     row = lax.broadcasted_iota(jnp.int32, (n, n), 0)
@@ -85,6 +111,7 @@
         mark = slice(heads * HEAD + h, heads * HEAD + h + 1)
         keep_ref[mark, :] = jnp.where(first, decays[0], decays[1])
         send_ref[mark, :] = jnp.where(first, decays[1], decays[0])
+    copy.wait()
 
 
 def pack_states(keep_ref, got_ref, out_ref):
@@ -149,7 +176,7 @@
     return centre * lax.rsqrt(spread + GROUP_EPS)
 
 
-def mix(inner_ref, query_ref, own_ref, got_ref, gate_ref, gain_ref, weight_ref, out_ref):
+def mix(inner_ref, query_ref, own_ref, got_ref, gate_ref, gain_ref, out_ref):
     heads = gate_ref.shape[1] // HEAD
     first = lax.axis_index("c") == 0
     mixed = []
@@ -164,39 +191,87 @@
         gate = gate_ref[:, cut].astype(F32)
         mixed.append((gate / (1.0 + jnp.exp(-gate)) * combined).astype(BF16))
     mixed = jnp.concatenate(mixed, axis=1)
-    attended = dot(mixed, weight_ref[...]).astype(BF16)
-    parts, rows, _ = out_ref.shape
-    for p in range(parts):
-        out_ref[p] = attended[p * rows : (p + 1) * rows, :]
-
-
-def finish_middle(in_ref, residual_ref, gain_ref, middle_ref, out_ref):
-    rows = middle_ref.shape[0]
-    start = pl.multiple_of(lax.axis_index("tp") * rows, rows)
-    attended = jnp.sum(in_ref[...].astype(F32), axis=0)
-    middle = (residual_ref[pl.ds(start, rows), :].astype(F32) + attended).astype(BF16)
-    middle_ref[...] = middle
-    values = middle.astype(F32)
-    scale = lax.rsqrt(jnp.mean(values * values, axis=1, keepdims=True) + NORM_EPS)
-    normed = (values * scale * gain_ref[...].astype(F32)).astype(BF16)
     for p in range(out_ref.shape[0]):
-        out_ref[p] = normed
-
-
-def convolved(pre, halo, taps, pair):
-    n = pre.shape[0] // pair
+        out_ref[p] = mixed
+
+
+def project(pair, tp, *refs):
+    mixed_ref, weight_ref, *refs = refs
+    near, refs = refs[: tp - 1], refs[tp - 1 :]
+    far, refs = refs[: tp - 1], refs[tp - 1 :]
+    residuals, refs = refs[:pair], refs[pair:]
+    gain_ref, normed_ref, middle_ref, first_ref, last_ref, scratch = refs
+    me, member, core = lax.axis_index("tp"), lax.axis_index("pr"), lax.axis_index("c")
+    n, width = mixed_ref.shape[1:]
+    half = width // 2
+    low = pl.multiple_of(core * half, half)
+    high = pl.multiple_of((1 - core) * half, half)
+    attended = 0.0
+    for d in range(tp):
+        parts = []
+        for s in range(pair):
+            i = lax.rem(member + s, pair) * tp + lax.rem(me - d + tp, tp)
+            if d == 0:
+                parts.append(mixed_ref[i])
+            else:
+                parts.append(
+                    jnp.concatenate(
+                        [mixed_ref[i, :, pl.ds(low, half)], mixed_ref[i, :, pl.ds(high, half)]],
+                        axis=1,
+                    )
+                )
+        rows = jnp.concatenate(parts, axis=0)
+        if d == 0:
+            weight = weight_ref[...]
+        else:
+            weight = jnp.concatenate([near[d - 1][...], far[d - 1][...]], axis=0)
+        attended = attended + dot(rows, weight)
+    firsts, lasts = [], []
+    for s in range(pair):
+        part = attended[s * n : (s + 1) * n, :]
+        middle = (residuals[s][...].astype(F32) + part).astype(BF16)
+        if s == 0:
+            scratch[...] = middle
+        values = middle.astype(F32)
+        scale = lax.rsqrt(jnp.mean(values * values, axis=1, keepdims=True) + NORM_EPS)
+        normed = values * scale * gain_ref[...].astype(F32)
+        normed_ref[s * n : (s + 1) * n, :] = normed.astype(BF16)
+        firsts.append(normed[0:1, :])
+        lasts.append(normed[n - 1 : n, :])
+    own = middle_ref.shape[0]
+    middle_ref[...] = scratch[pl.ds(pl.multiple_of(me * own, own), own), :]
+    fill = [jnp.zeros((first_ref.shape[0] - pair, first_ref.shape[1]), F32)]
+    first_ref[...] = jnp.concatenate(firsts + fill, axis=0).astype(BF16)
+    last_ref[...] = jnp.concatenate(lasts + fill, axis=0).astype(BF16)
+
+
+def convolved(pre, pair, taps):
+    n = (pre.shape[0] - 16) // pair
     row = lax.broadcasted_iota(jnp.int32, (n, pre.shape[1]), 0)
     spans = []
     for s in range(pair):
         x = pre[s * n : (s + 1) * n, :]
-        before = jnp.where(row == 0, halo[s : s + 1, :], pltpu.roll(x, 1, 0))
-        after = jnp.where(row == n - 1, halo[pair + s : pair + s + 1, :], pltpu.roll(x, n - 1, 0))
+        at = pair * n + s
+        before = jnp.where(row == 0, pre[at : at + 1, :], pltpu.roll(x, 1, 0))
+        after = jnp.where(row == n - 1, pre[at + 8 : at + 9, :], pltpu.roll(x, n - 1, 0))
         spans.append(taps[0:1] * before + taps[1:2] * x + taps[2:3] * after)
     return jnp.concatenate(spans, axis=0)
 
 
 def feed_forward(
-    pair, x_ref, halo_ref, gate_ref, up_ref, down_ref, gt_ref, ut_ref, out_ref, acc_ref
+    pair,
+    tp,
+    x_ref,
+    before_ref,
+    after_ref,
+    gate_ref,
+    up_ref,
+    down_ref,
+    gt_ref,
+    ut_ref,
+    out_ref,
+    rows_ref,
+    acc_ref,
 ):
     j = pl.program_id(0)
     block = gate_ref.shape[1]
@@ -204,35 +279,43 @@
     member = lax.axis_index("pr")
     at = pl.multiple_of(member * step + j * block, LANES)
     column = at + lax.broadcasted_iota(jnp.int32, (1, block), 1)
-    x, halo = x_ref[...], halo_ref[...]
+    count = x_ref.shape[0]
+
+    @pl.when(j == 0)
+    def _():
+        rows_ref[0:count, :] = x_ref[...]
+        rows_ref[count:, :] = jnp.concatenate([before_ref[...], after_ref[...]], axis=0)
 
     def branch(weight, taps):
-        pre = dot(x, weight).astype(BF16).astype(F32)
-        edge = dot(halo, weight).astype(BF16).astype(F32)
-        return convolved(pre, edge, taps, pair)
+        pre = dot(rows_ref[...], weight).astype(BF16).astype(F32)
+        return convolved(pre, pair, taps)
 
     gate = branch(gate_ref[...], gt_ref[:, pl.ds(at, block)].astype(F32))
     taps = jnp.where(column >= member * cols, ut_ref[:, pl.ds(at, block)].astype(F32), 0.0)
     up = branch(up_ref[...], taps)
     hidden = (gate / (1.0 + jnp.exp(-gate)) * up).astype(BF16)
     part = dot(hidden, down_ref[...], ((1,), (1,)))
+    last = pl.num_programs(0) - 1
 
     @pl.when(j == 0)
     def _():
         acc_ref[...] = part
 
-    @pl.when(j > 0)
+    @pl.when((j > 0) & (j < last))
     def _():
         acc_ref[...] += part
 
-    @pl.when(j == pl.num_programs(0) - 1)
+    @pl.when(j == last)
     def _():
-        parts, rows, _ = out_ref.shape
-        for p in range(parts):
-            out_ref[p] = acc_ref[p * rows : (p + 1) * rows, :].astype(BF16)
-
-
-def run_feed_forward(pair, peers, normed, halo, gathered, gate_taps, up_taps):
+        rows = out_ref.shape[1]
+        for s in range(pair):
+            for q in range(tp):
+                cut = slice((s * tp + q) * rows, (s * tp + q + 1) * rows)
+                whole = acc_ref[cut, :] + part[cut, :] if cols > block else part[cut, :]
+                out_ref[lax.rem(member + s, pair) * tp + q] = whole.astype(BF16)
+
+
+def run_feed_forward(pair, tp, normed, before, after, gathered, gate_taps, up_taps):
     depth, columns = gathered.shape
     cols = columns // 3
     block = 256
@@ -240,15 +323,17 @@
     whole = lambda a: pl.BlockSpec(a.shape, lambda j: (0,) * a.ndim)
     piece = lambda i: pl.BlockSpec((depth, block), lambda j, i=i: (0, i * steps + j))
     rows = normed.shape[0]
+    out = (pair * tp, rows // (pair * tp), depth)
     return pl.pallas_call(
-        lambda *refs: feed_forward(pair, *refs),
+        lambda *refs: feed_forward(pair, tp, *refs),
         grid=(steps,),
-        out_shape=shaped((peers, rows // peers, depth), BF16),
-        in_specs=[whole(normed), whole(halo), piece(0), piece(1), piece(2)]
+        out_shape=shaped(out, BF16),
+        in_specs=[whole(normed), whole(before), whole(after), piece(0), piece(1), piece(2)]
         + [whole(gate_taps), whole(up_taps)],
-        out_specs=pl.BlockSpec((peers, rows // peers, depth), lambda j: (0, 0, 0)),
-        scratch_shapes=[pltpu.VMEM((rows, depth), F32)],
-    )(normed, halo, gathered, gathered, gathered, gate_taps, up_taps)
+        out_specs=pl.BlockSpec(out, lambda j: (0, 0, 0)),
+        scratch_shapes=[pltpu.VMEM((rows + 16, depth), BF16), pltpu.VMEM((rows, depth), F32)],
+        compiler_params=pltpu.CompilerParams(vmem_limit_bytes=56 << 20),
+    )(normed, before, after, gathered, gathered, gathered, gate_taps, up_taps)
 
 
 def across(x, axes):
@@ -284,55 +369,75 @@
         gate_weight,
         up_weight,
         down_weight,
+        in_specs=[HBM] * 3,
+        out_specs=HBM,
+        scratch_shapes=[pltpu.SemaphoreType.DMA((3,))],
     )
     gathered = lax.all_gather(picked, SP, axis=0, tiled=True)
 
     marked = shaped((heads * HEAD + 8, HEAD), F32)
-    inner, query, keep, send = call(
+    inner, query, keep, send, half = call(
         local_retention,
-        (shaped((2, rows, width), F32), shaped((2, rows, width), BF16), marked, marked),
+        (
+            shaped((2, rows, width), F32),
+            shaped((2, rows, width), BF16),
+            marked,
+            marked,
+            shaped((width // 2, depth), BF16),
+        ),
         query_rows,
         key_rows,
         value_rows,
         log_decay,
+        out_weight,
+        in_specs=[VMEM] * 4 + [HBM],
+        out_specs=(VMEM,) * 4 + (HBM,),
+        scratch_shapes=[pltpu.SemaphoreType.DMA],
     )
     swap = [(0, 1), (1, 0)]
     got = lax.ppermute(send, "c", swap)
+    near = [
+        lax.ppermute(half, "tp", [(i, (i + d) % tp) for i in range(tp)]) for d in range(1, tp)
+    ]
+    far = [lax.ppermute(a, "c", swap) for a in near]
+    residuals = [residual] + [
+        lax.ppermute(residual, "pr", [((i + s) % pair, i) for i in range(pair)])
+        for s in range(1, pair)
+    ]
     used = heads * HEAD // chips
     message = call(pack_states, shaped((chips, used + 16, HEAD), BF16), keep, got)
     prefix = call(scan_states, shaped((chips, used, HEAD), BF16), across(message, "z"))
     state = shaped((heads * HEAD, HEAD), BF16)
     own, other = call(spread_states, (state, state), across(prefix, "z"), keep)
     entering = lax.ppermute(other, "c", swap)
-    attended = call(
+    mixed = call(
         mix,
-        shaped((tp, rows // tp, depth), BF16),
+        shaped((peers, rows, width), BF16),
         inner,
         query,
         own,
         entering,
         gate_rows,
         head_gain,
+    )
+    edge = shaped((8, depth), BF16)
+    normed, middle, first, last = call(
+        lambda *refs: project(pair, tp, *refs),
+        (shaped((pair * rows, depth), BF16), shaped((rows // tp, depth), BF16), edge, edge),
+        across(mixed, PEERS),
         out_weight,
-    )
-    middle, copies = call(
-        finish_middle,
-        (shaped((rows // tp, depth), BF16), shaped((peers, rows // tp, depth), BF16)),
-        across(attended, "tp"),
-        residual,
+        *near,
+        *far,
+        *residuals,
         norm_gain.reshape(1, depth),
-    )
-    normed = across(copies, PEERS).reshape(pair, rows, depth)
+        limit=60,
+        scratch_shapes=[pltpu.VMEM((rows, depth), BF16)],
+    )
     size = lax.axis_size("z") * lax.axis_size("c")
     onward = [(i, i + 1) for i in range(size - 1)]
-    back = [(j, i) for i, j in onward]
-    before = lax.ppermute(normed[:, rows - 1], SP, onward)
-    after = lax.ppermute(normed[:, 0], SP, back)
-    fill = jnp.zeros((16 - 2 * pair, depth), BF16)
-    halo = jnp.concatenate([before, after, fill], axis=0)
-    parts = run_feed_forward(
-        pair, peers, normed.reshape(pair * rows, depth), halo, gathered, gate_taps, up_taps
-    )
+    before = lax.ppermute(last, SP, onward)
+    after = lax.ppermute(first, SP, [(j, i) for i, j in onward])
+    parts = run_feed_forward(pair, tp, normed, before, after, gathered, gate_taps, up_taps)
     summed = across(parts, PEERS).astype(F32).sum(axis=0)
     return (middle.astype(F32) + summed).astype(BF16)
 

time: 160 us -> 157 us (0.981)
  blocking collectives: 71.6 us -> 36.1 us
  starting transfers between devices: 35.4 us -> 53.8 us
  local copies, waits for them, and re-layouts: 3.51 us -> 13.8 us
  waiting for transfers between devices: 10.7 us -> 20.9 us
  Pallas kernels: 23.1 us -> 17 us
    all_to_all x4 -> x2, blocking collectives: 71.6 us -> 36.1 us  [across(): return lax.all_to_all(x, axes, 0, 0, tiled=True)]
    ppermute x2 -> x9, waiting for transfers between devices: 0.69 us -> 12.5 us  [the longest x1 11.1 us: shards(): lax.ppermute(residual, 'pr', [((i + s) % pair, i) for i in range(pair)])]
    unnamed x12 -> x42, local copies, waits for them, and re-layouts: 2.11 us -> 12.5 us
    ppermute x2 -> x9, starting transfers between devices: 7.85 us -> 17.3 us  [the longest x3 5.29 us: shards(): lax.ppermute(half, 'tp', [(i, (i + d) % tp) for i in range(tp)])]
    all_to_all x1 -> x2, starting transfers between devices: 4.26 us -> 13.3 us  [across(): return lax.all_to_all(x, axes, 0, 0, tiled=True)]
    pallas_call x8, Pallas kernels: 23.1 us -> 17 us  [the longest x1 8.6 us: run_feed_forward(): pl.pallas_call(lambda *refs: feed_forward(pair, tp, *refs), grid=(steps,)...]
    all_to_all x1 -> x2, waiting for transfers between devices: 7.64 us -> 6.49 us  [across(): return lax.all_to_all(x, axes, 0, 0, tiled=True)]
  transfers between devices with their start and end apart: 6 -> 14, of which waited for: 4 -> 5; matrix products, arithmetic and copies ran while one was open for 1% -> 1% of each run, Pallas kernels for 8% -> 5%
where the time goes in v2:
time: 157 us; the launch traced here: 156 us
  starting transfers between devices  53.8 us (34%)
  blocking collectives  36.1 us (23%)
  waiting for transfers between devices  20.9 us (13%)
  Pallas kernels  17 us (11%)
  local copies, waits for them, and re-layouts  13.8 us (9%)
  between operations  13.6 us (9%)
    all_to_all x2, blocking collectives, across(): return lax.all_to_all(x, axes, 0, 0, tiled=True)  36.1 us
    ppermute x1, starting transfers between devices, shards(): got = lax.ppermute(send, 'c', swap)  20.5 us
    all_to_all x2, starting transfers between devices, across(): return lax.all_to_all(x, axes, 0, 0, tiled=True)  13.3 us
    unnamed x42, local copies, waits for them, and re-layouts  12.5 us
    ppermute x1, waiting for transfers between devices, shards(): lax.ppermute(residual, 'pr', [((i + s) % pair, i) for i in range(pair)])  11.1 us
    pallas_call x1, Pallas kernels, run_feed_forward(): pl.pallas_call(lambda *refs: feed_forward(pair, tp, *refs), grid=(steps,)...  8.6 us
    pallas_call x7, Pallas kernels, call(): pl.pallas_call(body, out_shape=outs, compiler_params=pltpu.CompilerParams...  8.43 us
    all_to_all x2, waiting for transfers between devices, across(): return lax.all_to_all(x, axes, 0, 0, tiled=True)  6.49 us
  transfers between devices with their start and end apart: 14, of which 5 were waited for; matrix products, arithmetic and copies ran while one was open for 1% of the time, Pallas kernels for 5%

profile of v2, /device:TPU:33, one launch (start us, length us, event | category | flops | bytes accessed | tf_op | source)
XLA Modules:
  0.0 156.0 jit_solution(2915926837263905886)
XLA Ops:
  6.5 0.0 all-gather.2.cloned.1.call-start
  6.6 0.0 copy-start.1
  6.6 0.9 copy-done.1
  7.5 0.0 copy-start.2
  7.5 0.9 copy-done.2
  8.4 0.9 copy-done.3
  9.3 0.7 shard_map.142
  10.1 0.1 all-gather.2.cloned.1.call-update
  10.1 0.0 copy-start
  10.1 1.2 copy-done
  11.4 0.8 copy-done.4
  12.2 0.8 copy-done.5
  13.0 0.8 copy-done.6
  13.9 0.7 copy-done.8
  14.6 0.6 shard_map.136
  15.2 20.5 %collective-permute-start = (f32[264,128]{1,0:T(8,128)S(1)}, f32[264,128]{1,0:T(8,128)S(1)}, u32[]{:S(2)}, u32[]{:S(2)}) collective-permute-start(f32[264,128]{1,0:T(8,128)S(1)} %get-tuple-element.19), channel_id=1, source_target_pairs={{0,4},{4,0},{1,5},{5,1},{2,6},{6,2},{3,7},{7,3},{8,12},{12,8},{9,1... | collective-permute-start | bytes 405512 | tf_op jit(solution)/shard_map/ppermute | solution.py:398
  35.7 1.0 collective-permute-done.got_ref
  36.7 17.4 %all_to_all.20.in_ref = bf16[16,32,128]{2,1,0:T(8,128)(2,1)S(1)} all-to-all(bf16[16,32,128]{2,1,0:T(8,128)(2,1)S(1)} %shard_map.137), channel_id=1, replica_groups=mesh['pg'=1,'pr'=2,'z'=16,'c'=2,'tp'=4] {'z'}, dimensions={0} | all-to-all | bytes 262144 | tf_op jit(solution)/shard_map/all_to_all | solution.py:340
  54.1 0.7 shard_map.138
  54.8 7.3 %all-to-all-start.1 = ((bf16[16,16,128]{2,1,0:T(8,128)(2,1)}), bf16[16,16,128]{2,1,0:T(8,128)(2,1)S(1)}, u32[]{:S(2)}, u32[]{:S(2)}) async-start(bf16[16,16,128]{2,1,0:T(8,128)(2,1)} %shard_map.138), calls=%async_computation.1 | async-start | bytes 131072 | tf_op jit(solution)/shard_map/all_to_all | solution.py:340
  62.1 1.5 collective-permute-start.2
  63.6 2.8 %collective-permute-start.3 = (bf16[128,2048]{1,0:T(8,128)(2,1)S(1)}, bf16[128,2048]{1,0:T(8,128)(2,1)S(1)}, u32[]{:S(2)}, u32[]{:S(2)}) collective-permute-start(bf16[128,2048]{1,0:T(8,128)(2,1)S(1)} %get-tuple-element.22), channel_id=1, source_target_pairs={{0,2},{1,3},{2,0},{3,1},{4,6},{5,7},{6,4},{7,5},{8,10},{9,11},{10,... | collective-permute-start | bytes 1572872 | tf_op jit(solution)/shard_map/ppermute | solution.py:400
  66.4 1.0 collective-permute-start.4
  67.4 6.5 %all-to-all-done.1.in_ref = bf16[16,16,128]{2,1,0:T(8,128)(2,1)S(1)} async-done(((bf16[16,16,128]{2,1,0:T(8,128)(2,1)}), bf16[16,16,128]{2,1,0:T(8,128)(2,1)S(1)}, u32[]{:S(2)}, u32[]{:S(2)}) %all-to-all-start.1) | async-done | bytes 65568 | tf_op jit(solution)/shard_map/all_to_all | solution.py:340
  73.9 2.8 %collective-permute-start.1 = (bf16[256,128]{1,0:T(8,128)(2,1)S(1)}, bf16[256,128]{1,0:T(8,128)(2,1)S(1)}, u32[]{:S(2)}, u32[]{:S(2)}) collective-permute-start(bf16[256,128]{1,0:T(8,128)(2,1)S(1)} %get-tuple-element.21), channel_id=1, source_target_pairs={{0,4},{4,0},{1,5},{5,1},{2,6},{6,2},{3,7},{7,3},{8,12},{12,8},{9,1... | collective-permute-start | bytes 196616 | tf_op jit(solution)/shard_map/ppermute | solution.py:412
  76.7 0.9 collective-permute-done.1.got_ref
  77.6 0.8 copy-done.7
  78.4 0.7 copy-done.9
  79.1 1.2 shard_map.140
  80.3 6.0 %all-to-all-start.2 = ((bf16[8,128,256]{2,1,0:T(8,128)(2,1)}), bf16[8,128,256]{2,1,0:T(8,128)(2,1)S(1)}, u32[]{:S(2)}, u32[]{:S(2)}) async-start(bf16[8,128,256]{2,1,0:T(8,128)(2,1)} %shard_map.140), calls=%async_computation.2 | async-start | bytes 1048576 | tf_op jit(solution)/shard_map/all_to_all | solution.py:340
  86.3 1.5 collective-permute-start.8
  87.7 0.0 collective-permute-done.2.refs_2_
  87.7 1.2 collective-permute-start.5
  88.9 0.0 collective-permute-done.3.refs_3_
  88.9 1.6 %collective-permute-start.6 = (bf16[128,2048]{1,0:T(8,128)(2,1)S(1)}, bf16[128,2048]{1,0:T(8,128)(2,1)S(1)}, u32[]{:S(2)}, u32[]{:S(2)}) collective-permute-start(bf16[128,2048]{1,0:T(8,128)(2,1)S(1)} %collective-permute-done.3.refs_3_), channel_id=1, source_target_pairs={{0,4},{4,0},{1,5},{5,1},{2,6},{6,2},{3,7},{7,3},{8,12},{12,8},{9,1... | collective-permute-start | bytes 1572872 | tf_op jit(solution)/shard_map/ppermute | solution.py:402
  90.5 0.0 collective-permute-done.4.refs_4_
  90.5 2.0 %collective-permute-start.7 = (bf16[128,2048]{1,0:T(8,128)(2,1)S(1)}, bf16[128,2048]{1,0:T(8,128)(2,1)S(1)}, u32[]{:S(2)}, u32[]{:S(2)}) collective-permute-start(bf16[128,2048]{1,0:T(8,128)(2,1)S(1)} %collective-permute-done.4.refs_4_), channel_id=1, source_target_pairs={{0,4},{4,0},{1,5},{5,1},{2,6},{6,2},{3,7},{7,3},{8,12},{12,8},{9,1... | collective-permute-start | bytes 1572872 | tf_op jit(solution)/shard_map/ppermute | solution.py:402
  92.5 1.3 reshape.3.refs_10_
  93.8 11.1 %collective-permute-done.8.refs_9_ = bf16[128,2048]{1,0:T(8,128)(2,1)S(1)} collective-permute-done((bf16[128,2048]{1,0:T(8,128)(2,1)}, bf16[128,2048]{1,0:T(8,128)(2,1)S(1)}, u32[]{:S(2)}, u32[]{:S(2)}) %collective-permute-start.8) | collective-permute-done | bytes 524320 | tf_op jit(solution)/shard_map/ppermute | solution.py:404
  104.9 0.0 collective-permute-done.5.refs_5_
  104.9 0.0 collective-permute-done.6.refs_6_
  105.0 0.8 copy-done.15
  105.8 0.8 copy-done.16
  106.6 0.0 collective-permute-done.7.refs_7_
  106.6 0.0 all-to-all-done.2.refs_0_
  106.6 0.0 copy-done.11
  106.6 0.0 copy-done.12
  106.6 0.0 copy-done.13
  106.7 0.0 copy-done.14
  106.7 0.7 copy-done.17
  107.4 0.8 copy-done.10
  108.2 5.2 %shard_map.141 = (bf16[256,2048]{1,0:T(8,128)(2,1)}, bf16[32,2048]{1,0:T(8,128)(2,1)}, bf16[8,2048]{1,0:T(8,128)(2,1)}, bf16[8,2048]{1,0:T(8,128)(2,1)}) custom-call(bf16[8,128,256]{2,1,0:T(8,128)(2,1)} %copy-done.10, bf16[256,2048]{1,0:T(8,128)(2,1)} %refs_1_.2, bf16[128,2048]{1,0:T(8,128)(2,1)} %copy-done.11, bf16[128,2048]{1,0:T(8,128)(2,1)} %copy-done.12, ...), custom_call_target="tpu_custom_call" | custom-call | tf_op jit(solution)/shard_map/pallas_call | solution.py:28
  113.4 3.4 %collective-permute-start.10 = (bf16[8,2048]{1,0:T(8,128)(2,1)}, bf16[8,2048]{1,0:T(8,128)(2,1)S(1)}, u32[]{:S(2)}, u32[]{:S(2)}) collective-permute-start(bf16[8,2048]{1,0:T(8,128)(2,1)} %get-tuple-element.26), channel_id=1, source_target_pairs={{4,0},{8,4},{12,8},{16,12},{20,16},{24,20},{28,24},{32,28},{36,32}... | collective-permute-start | bytes 98312 | tf_op jit(solution)/shard_map/ppermute | solution.py:439
  116.9 2.3 %collective-permute-start.9 = (bf16[8,2048]{1,0:T(8,128)(2,1)}, bf16[8,2048]{1,0:T(8,128)(2,1)S(1)}, u32[]{:S(2)}, u32[]{:S(2)}) collective-permute-start(bf16[8,2048]{1,0:T(8,128)(2,1)} %get-tuple-element.25), channel_id=1, source_target_pairs={{0,4},{4,8},{8,12},{12,16},{16,20},{20,24},{24,28},{28,32},{32,36}... | collective-permute-start | bytes 98312 | tf_op jit(solution)/shard_map/ppermute | solution.py:438
  119.2 0.0 collective-permute-done.10.refs_2_
  119.2 0.0 copy-start.19
  119.2 1.3 collective-permute-done.9.refs_1_
  120.5 0.0 copy-done.19
  120.5 0.6 copy-done.20
  121.1 8.6 %shard_map.143 = bf16[8,32,2048]{2,1,0:T(8,128)(2,1)} custom-call(bf16[256,2048]{1,0:T(8,128)(2,1)} %get-tuple-element.24.refs_0_, bf16[8,2048]{1,0:T(8,128)(2,1)} %copy-done.20, bf16[8,2048]{1,0:T(8,128)(2,1)} %copy-done.19, bf16[2048,2304]{1,0:T(8,128)(2,1)} %all-gather.2.cloned.1.call-done.refs_3_.refs_4_.refs_5_, ...), custom_call_target="tpu_custom_call" | custom-call | tf_op jit(solution)/shard_map/pallas_call | solution.py:327
  129.7 18.6 %all_to_all.21 = bf16[8,32,2048]{2,1,0:T(8,128)(2,1)S(1)} all-to-all(bf16[8,32,2048]{2,1,0:T(8,128)(2,1)} %shard_map.143), channel_id=1, replica_groups=mesh['pg'=1,'pr'=2,'z'=16,'c'=2,'tp'=4] {'pr','tp'}, dimensions={0} | all-to-all | bytes 2097152 | tf_op jit(solution)/shard_map/all_to_all | solution.py:340
  148.4 0.1 convert_reduce_fusion
  148.5 0.0 copy-done.18
  148.5 0.7 add_convert_fusion
  (20 shorter events, 0.1 us)
Async XLA Ops:
  6.5 113.9 %all-gather.2.cloned.1.call-start = ((), (), s32[]{:S(2)}) async-start(), calls=%async_computation.4 | async-start | bytes 9732096 | tf_op jit(solution)/shard_map/all_gather | solution.py:376
  6.6 0.9 copy-start.1
  7.5 0.9 copy-start.2
  8.4 0.9 copy-start.3
  10.1 1.2 copy-start
  11.4 0.8 copy-start.4
  12.2 0.8 copy-start.5
  13.0 0.8 copy-start.6
  13.9 0.7 copy-start.8
  15.2 21.5 %collective-permute-start = (f32[264,128]{1,0:T(8,128)S(1)}, f32[264,128]{1,0:T(8,128)S(1)}, u32[]{:S(2)}, u32[]{:S(2)}) collective-permute-start(f32[264,128]{1,0:T(8,128)S(1)} %get-tuple-element.19), channel_id=1, source_target_pairs={{0,4},{4,0},{1,5},{5,1},{2,6},{6,2},{3,7},{7,3},{8,12},{12,8},{9,1... | collective-permute-start | bytes 405512 | tf_op jit(solution)/shard_map/ppermute | solution.py:398
  54.8 19.1 %all-to-all-start.1 = ((bf16[16,16,128]{2,1,0:T(8,128)(2,1)}), bf16[16,16,128]{2,1,0:T(8,128)(2,1)S(1)}, u32[]{:S(2)}, u32[]{:S(2)}) async-start(bf16[16,16,128]{2,1,0:T(8,128)(2,1)} %shard_map.138), calls=%async_computation.1 | async-start | bytes 131072 | tf_op jit(solution)/shard_map/all_to_all | solution.py:340
  62.1 25.6 %collective-permute-start.2 = (bf16[128,2048]{1,0:T(8,128)(2,1)S(1)}, bf16[128,2048]{1,0:T(8,128)(2,1)S(1)}, u32[]{:S(2)}, u32[]{:S(2)}) collective-permute-start(bf16[128,2048]{1,0:T(8,128)(2,1)S(1)} %get-tuple-element.22), channel_id=1, source_target_pairs={{0,1},{1,2},{2,3},{3,0},{4,5},{5,6},{6,7},{7,4},{8,9},{9,10},{10,1... | collective-permute-start | bytes 1572872 | tf_op jit(solution)/shard_map/ppermute | solution.py:400
  63.6 25.3 %collective-permute-start.3 = (bf16[128,2048]{1,0:T(8,128)(2,1)S(1)}, bf16[128,2048]{1,0:T(8,128)(2,1)S(1)}, u32[]{:S(2)}, u32[]{:S(2)}) collective-permute-start(bf16[128,2048]{1,0:T(8,128)(2,1)S(1)} %get-tuple-element.22), channel_id=1, source_target_pairs={{0,2},{1,3},{2,0},{3,1},{4,6},{5,7},{6,4},{7,5},{8,10},{9,11},{10,... | collective-permute-start | bytes 1572872 | tf_op jit(solution)/shard_map/ppermute | solution.py:400
  66.4 24.1 %collective-permute-start.4 = (bf16[128,2048]{1,0:T(8,128)(2,1)S(1)}, bf16[128,2048]{1,0:T(8,128)(2,1)S(1)}, u32[]{:S(2)}, u32[]{:S(2)}) collective-permute-start(bf16[128,2048]{1,0:T(8,128)(2,1)S(1)} %get-tuple-element.22), channel_id=1, source_target_pairs={{0,3},{1,0},{2,1},{3,2},{4,7},{5,4},{6,5},{7,6},{8,11},{9,8},{10,9... | collective-permute-start | bytes 1572872 | tf_op jit(solution)/shard_map/ppermute | solution.py:400
  73.9 3.7 %collective-permute-start.1 = (bf16[256,128]{1,0:T(8,128)(2,1)S(1)}, bf16[256,128]{1,0:T(8,128)(2,1)S(1)}, u32[]{:S(2)}, u32[]{:S(2)}) collective-permute-start(bf16[256,128]{1,0:T(8,128)(2,1)S(1)} %get-tuple-element.21), channel_id=1, source_target_pairs={{0,4},{4,0},{1,5},{5,1},{2,6},{6,2},{3,7},{7,3},{8,12},{12,8},{9,1... | collective-permute-start | bytes 196616 | tf_op jit(solution)/shard_map/ppermute | solution.py:412
  77.6 0.8 copy-start.7
  78.4 0.7 copy-start.9
  80.3 26.3 %all-to-all-start.2 = ((bf16[8,128,256]{2,1,0:T(8,128)(2,1)}), bf16[8,128,256]{2,1,0:T(8,128)(2,1)S(1)}, u32[]{:S(2)}, u32[]{:S(2)}) async-start(bf16[8,128,256]{2,1,0:T(8,128)(2,1)} %shard_map.140), calls=%async_computation.2 | async-start | bytes 1048576 | tf_op jit(solution)/shard_map/all_to_all | solution.py:340
  86.3 18.7 %collective-permute-start.8 = (bf16[128,2048]{1,0:T(8,128)(2,1)}, bf16[128,2048]{1,0:T(8,128)(2,1)S(1)}, u32[]{:S(2)}, u32[]{:S(2)}) collective-permute-start(bf16[128,2048]{1,0:T(8,128)(2,1)} %refs_8_.1), channel_id=1, source_target_pairs={{128,0},{0,128},{129,1},{1,129},{130,2},{2,130},{131,3},{3,131},{1... | collective-permute-start | bytes 1572872 | tf_op jit(solution)/shard_map/ppermute | solution.py:404
  87.7 18.9 %copy-start.11 = (bf16[128,2048]{1,0:T(8,128)(2,1)}, bf16[128,2048]{1,0:T(8,128)(2,1)S(1)}, u32[]{:S(2)}) copy-start(bf16[128,2048]{1,0:T(8,128)(2,1)S(1)} %collective-permute-done.2.refs_2_) | copy-start | bytes 1572868
  87.7 17.2 %collective-permute-start.5 = (bf16[128,2048]{1,0:T(8,128)(2,1)S(1)}, bf16[128,2048]{1,0:T(8,128)(2,1)S(1)}, u32[]{:S(2)}, u32[]{:S(2)}) collective-permute-start(bf16[128,2048]{1,0:T(8,128)(2,1)S(1)} %collective-permute-done.2.refs_2_), channel_id=1, source_target_pairs={{0,4},{4,0},{1,5},{5,1},{2,6},{6,2},{3,7},{7,3},{8,12},{12,8},{9,1... | collective-permute-start | bytes 1572872 | tf_op jit(solution)/shard_map/ppermute | solution.py:402
  88.9 17.7 %copy-start.12 = (bf16[128,2048]{1,0:T(8,128)(2,1)}, bf16[128,2048]{1,0:T(8,128)(2,1)S(1)}, u32[]{:S(2)}) copy-start(bf16[128,2048]{1,0:T(8,128)(2,1)S(1)} %collective-permute-done.3.refs_3_) | copy-start | bytes 1572868
  88.9 16.0 %collective-permute-start.6 = (bf16[128,2048]{1,0:T(8,128)(2,1)S(1)}, bf16[128,2048]{1,0:T(8,128)(2,1)S(1)}, u32[]{:S(2)}, u32[]{:S(2)}) collective-permute-start(bf16[128,2048]{1,0:T(8,128)(2,1)S(1)} %collective-permute-done.3.refs_3_), channel_id=1, source_target_pairs={{0,4},{4,0},{1,5},{5,1},{2,6},{6,2},{3,7},{7,3},{8,12},{12,8},{9,1... | collective-permute-start | bytes 1572872 | tf_op jit(solution)/shard_map/ppermute | solution.py:402
  90.5 16.1 %copy-start.13 = (bf16[128,2048]{1,0:T(8,128)(2,1)}, bf16[128,2048]{1,0:T(8,128)(2,1)S(1)}, u32[]{:S(2)}) copy-start(bf16[128,2048]{1,0:T(8,128)(2,1)S(1)} %collective-permute-done.4.refs_4_) | copy-start | bytes 1572868
  90.5 16.1 %collective-permute-start.7 = (bf16[128,2048]{1,0:T(8,128)(2,1)S(1)}, bf16[128,2048]{1,0:T(8,128)(2,1)S(1)}, u32[]{:S(2)}, u32[]{:S(2)}) collective-permute-start(bf16[128,2048]{1,0:T(8,128)(2,1)S(1)} %collective-permute-done.4.refs_4_), channel_id=1, source_target_pairs={{0,4},{4,0},{1,5},{5,1},{2,6},{6,2},{3,7},{7,3},{8,12},{12,8},{9,1... | collective-permute-start | bytes 1572872 | tf_op jit(solution)/shard_map/ppermute | solution.py:402
  104.9 1.7 %copy-start.14 = (bf16[128,2048]{1,0:T(8,128)(2,1)}, bf16[128,2048]{1,0:T(8,128)(2,1)S(1)}, u32[]{:S(2)}) copy-start(bf16[128,2048]{1,0:T(8,128)(2,1)S(1)} %collective-permute-done.8.refs_9_) | copy-start | bytes 1572868
  104.9 0.9 copy-start.15
  105.8 0.8 copy-start.16
  106.6 0.8 copy-start.17
  107.4 0.8 copy-start.10
  113.4 5.8 %collective-permute-start.10 = (bf16[8,2048]{1,0:T(8,128)(2,1)}, bf16[8,2048]{1,0:T(8,128)(2,1)S(1)}, u32[]{:S(2)}, u32[]{:S(2)}) collective-permute-start(bf16[8,2048]{1,0:T(8,128)(2,1)} %get-tuple-element.26), channel_id=1, source_target_pairs={{4,0},{8,4},{12,8},{16,12},{20,16},{24,20},{28,24},{32,28},{36,32}... | collective-permute-start | bytes 98312 | tf_op jit(solution)/shard_map/ppermute | solution.py:439
  116.9 3.6 %collective-permute-start.9 = (bf16[8,2048]{1,0:T(8,128)(2,1)}, bf16[8,2048]{1,0:T(8,128)(2,1)S(1)}, u32[]{:S(2)}, u32[]{:S(2)}) collective-permute-start(bf16[8,2048]{1,0:T(8,128)(2,1)} %get-tuple-element.25), channel_id=1, source_target_pairs={{0,4},{4,8},{8,12},{12,16},{16,20},{20,24},{24,28},{28,32},{32,36}... | collective-permute-start | bytes 98312 | tf_op jit(solution)/shard_map/ppermute | solution.py:438
  119.2 1.3 copy-start.19
  120.5 0.6 copy-start.20
  121.1 27.4 %copy-start.18 = (bf16[32,2048]{1,0:T(8,128)(2,1)S(1)}, bf16[32,2048]{1,0:T(8,128)(2,1)}, u32[]{:S(2)}) copy-start(bf16[32,2048]{1,0:T(8,128)(2,1)} %get-tuple-element.23) | copy-start | bytes 393220
Sparse Core Ops, SparseCore 0:
  10.3 100.6 all-gather.1
